TPU v7x, 128 devices: a whole 4x4x4 slice. The times are simulated.
128 devices in a mesh: sp: 32 (over z, y, core), tp: 4 (over x).
Axes of the slice: x: 4, y: 4, z: 4, core: 2. Of those that a mesh axis runs over, the one named last changes fastest.
Arguments:
- queries: bfloat16 [8192, 2048], P('sp', 'tp'), may hold values from -6 to 6
- key_value: bfloat16 [8192, 4, 128], P('sp', 'tp'), may hold values from -12 to 12
- break_bias: bfloat16 [8192, 32], P('sp', 'tp'), may hold values from -13 to 0
- stream: bfloat16 [8192, 2048], P(('sp', 'tp')), may hold values from -6 to 6
- out_proj: bfloat16 [2048, 2048], replicated, may hold values from -0.125 to 0.125
- ffn_gain: float32 [2048], replicated, may hold values from 0.1 to 1.9
- routes: int32 [8192, 4], P(('sp', 'tp')), may hold values from 0 to 127, all different within a row; in each aligned block of 64 rows (0 to 63, 64 to 127, ...) at most 4 rows name the same one
- route_score: float32 [8192, 4], P(('sp', 'tp')), may hold values from 0.05 to 1
- expert_gate: bfloat16 [128, 2048, 512], P(('sp', 'tp')), may hold values from -0.125 to 0.125
- expert_up: bfloat16 [128, 2048, 512], P(('sp', 'tp')), may hold values from -0.125 to 0.125
- expert_down: bfloat16 [128, 512, 2048], P(('sp', 'tp')), may hold values from -0.25 to 0.25
- shared_gate: bfloat16 [2048, 512], replicated, may hold values from -0.125 to 0.125
- shared_up: bfloat16 [2048, 512], replicated, may hold values from -0.125 to 0.125
- shared_down: bfloat16 [512, 2048], replicated, may hold values from -0.25 to 0.25
Outputs:
- layer_out: bfloat16 [8192, 2048], P(('sp', 'tp'))
Inputs may be any that keep to these rules, and one draw needn't show every extreme that they name: `routes`: each row names 4 different experts. In each aligned block of 64 rows (the rows of one device) no expert is named by more than 4 rows, a bound that some block reaches.
All inputs are finite; a program needn't handle non-finite values.
Results may differ from a plain program's by a relative error of at most 0.015.
Values may be sent and summed in bfloat16 or wider, within the bound.
A program may use at most 128 MiB of HBM per device.

v0:
```python
import functools

import jax
import jax.numpy as jnp
import numpy as np
from jax import lax
from jax.experimental import pallas as pl
from jax.experimental.pallas import tpu as pltpu
from jax.sharding import PartitionSpec as P

GROUP = 8
LOG2E = 1.4426950408889634


def schedule(blocks, tiles, group):
    half = blocks // 2
    rows = []
    give = []
    for i in range(half):
        best = min(range(0, tiles // 2 + 1), key=lambda n: max(tiles * (i + 1) + n * (blocks - i), (tiles - n) * (blocks - i)))
        give.append(best)
    for i in range(blocks):
        n = give[min(i, blocks - 1 - i)]
        if i < half:
            slots = [(s, i) for s in range(tiles)] + [(tiles + s, blocks - 1 - i) for s in range(n)]
        else:
            slots = [(s, i) for s in range(n, tiles)]
        diag = [(s, q) for s, q in slots]
        main = []
        depth = max(q for _, q in slots)
        for back in range(1, depth + 1):
            for s, q in slots:
                if q - back >= 0:
                    main.append((s, q - back))
        rows.append((diag, main))
    spare = tiles + tiles // 2
    ld = max(-(-len(d) // group) for d, _ in rows)
    lm = max(-(-len(m) // group) for _, m in rows)
    table = np.zeros((blocks, 2 + 2 * group * (ld + lm)), np.int32)
    for i, (diag, main) in enumerate(rows):
        nd, nm = -(-len(diag) // group), -(-len(main) // group)
        diag = diag + [(spare, 0)] * (group * ld - len(diag))
        main = main + [(spare, 0)] * (group * lm - len(main))
        table[i, 0], table[i, 1] = nd, nm
        table[i, 2:] = np.array(diag + main).reshape(-1)
    return table, np.array(give), ld, lm


def attend_kernel(group, ld, tab, q_ref, kv_ref, tri_ref, out_ref, qs, acc, carry):
    nt = out_ref.shape[0] // 32
    f32, bf16 = jnp.float32, jnp.bfloat16
    head_lane = lax.broadcasted_iota(jnp.int32, (32, 16), 1)
    c_hi = float(np.asarray(LOG2E, jnp.bfloat16))
    c_lo = float(np.float32(LOG2E - c_hi))

    def build(s, _):
        q = q_ref[pl.ds(s * 32, 32), :].astype(f32) * (0.125 * LOG2E)
        hi = q.astype(bf16)
        lo = (q - hi.astype(f32)).astype(bf16)
        for h in range(8):
            tail = jnp.where(head_lane == h, c_hi, jnp.where(head_lane == h + 8, c_lo, 0.0)).astype(bf16)
            qs[s, pl.ds(h * 32, 32), :] = jnp.concatenate([hi[:, 64 * h:64 * h + 64], lo[:, 64 * h:64 * h + 64], tail], axis=1)
        return 0

    lax.fori_loop(0, nt, build, 0)
    qs[nt] = jnp.zeros_like(qs[nt])
    acc[...] = jnp.zeros_like(acc)
    carry[...] = jnp.zeros_like(carry)
    lane = lax.broadcasted_iota(jnp.int32, (128, 128), 1)

    def step(base, masked):
        for g in range(group):
            slot = tab[base + 2 * g]
            chunk = tab[base + 2 * g + 1]
            key = jnp.concatenate([kv_ref[chunk, 0:64, :], kv_ref[chunk, 0:80, :]], axis=0)
            z = jnp.dot(qs[slot], key, preferred_element_type=f32)
            if masked:
                row = lax.broadcasted_iota(jnp.int32, (256, 256), 0) % 32 + (slot % 8) * 32
                col = lax.broadcasted_iota(jnp.int32, (256, 256), 1)
                z = jnp.where(col < row, z, -1e30)
            sp = jnp.maximum(z, lax.log2(1.0 + jnp.exp2(jnp.minimum(z, 126.0))))
            u = z - sp
            sums = jnp.dot(sp.astype(bf16), tri_ref[...], preferred_element_type=f32)
            before = carry[slot]
            w = jnp.exp2(u - sums[:, :256] - jnp.concatenate([before, before], axis=1)).astype(bf16)
            carry[slot] = before + sums[:, 256:]
            vx = kv_ref[chunk, 80:144, :]
            v = jnp.concatenate([vx[:, :128], vx[:, 128:]], axis=0)
            zero = jnp.zeros_like(v)
            both = jnp.concatenate([jnp.where(lane < 64, v, zero), jnp.where(lane < 64, zero, v)], axis=0)
            acc[slot] += jnp.dot(w, both, preferred_element_type=f32)

    def diag_step(j, _):
        step(2 + 2 * group * j, True)
        return 0

    def main_step(j, _):
        step(2 + 2 * group * (ld + j), False)
        return 0

    lax.fori_loop(0, tab[0], diag_step, 0)
    lax.fori_loop(0, tab[1], main_step, 0)

    def finish(s, _):
        for p in range(4):
            pair = []
            for h in (2 * p, 2 * p + 1):
                a = acc[s, pl.ds(h * 32, 32), :]
                pair.append(a[:, :64] + a[:, 64:])
            out_ref[pl.ds(s * 32, 32), pl.ds(128 * p, 128)] = jnp.concatenate(pair, axis=1).astype(bf16)
        return 0

    lax.fori_loop(0, nt, finish, 0)


def triangle():
    t = np.zeros((256, 384), np.float32)
    t[:, :256] = np.tril(np.ones((256, 256)), -1)
    t[:, 256:] = 1.0
    return t


def attend(tab, q_all, kv, group, ld):
    nt = q_all.shape[0] // 32
    vm = pl.BlockSpec(memory_space=pltpu.VMEM)
    return pl.pallas_call(
        functools.partial(attend_kernel, group, ld),
        out_shape=jax.ShapeDtypeStruct(q_all.shape, jnp.bfloat16),
        in_specs=[pl.BlockSpec(memory_space=pltpu.SMEM), vm, vm, vm],
        out_specs=vm,
        scratch_shapes=[pltpu.VMEM((nt + 1, 256, 144), jnp.bfloat16), pltpu.VMEM((nt + 1, 256, 128), jnp.float32), pltpu.VMEM((nt + 1, 256, 128), jnp.float32)],
        compiler_params=pltpu.CompilerParams(vmem_limit_bytes=48 * 1024 * 1024),
        name="attend",
    )(tab, q_all, kv, jnp.asarray(triangle(), jnp.bfloat16))


def pack_kv(key_value, bias):
    kt = key_value[:, :64].T
    b = bias.T
    v = key_value[:, 64:]
    left = jnp.concatenate([v[0:64], v[128:192]], axis=1)
    right = jnp.concatenate([v[64:128], v[192:256]], axis=1)
    return jnp.concatenate([kt, b, b, jnp.concatenate([left, right], axis=1)], axis=0)


def from_everyone(array, axis):
    copies = jnp.broadcast_to(array, (lax.axis_size(axis), *array.shape))
    return lax.all_to_all(copies, axis, split_axis=0, concat_axis=0, tiled=True)


def expert_rows(arrived, w_gate, w_up, w_down):
    gate_part = jnp.einsum("snd,df->snf", arrived, w_gate, preferred_element_type=jnp.float32)
    up_part = jnp.einsum("snd,df->snf", arrived, w_up, preferred_element_type=jnp.float32)
    inner = (jax.nn.silu(gate_part) * up_part).astype(jnp.bfloat16)
    return jnp.einsum("snf,fd->snd", inner, w_down, preferred_element_type=jnp.float32).astype(
        jnp.bfloat16
    )


def body(
    queries,
    key_value,
    break_bias,
    stream,
    out_proj,
    ffn_gain,
    routes,
    route_score,
    expert_gate,
    expert_up,
    expert_down,
    shared_gate,
    shared_up,
    shared_down,
):
    table, give, diag_groups, _ = schedule(lax.axis_size("sp"), queries.shape[0] // 32, GROUP)
    blocks = lax.axis_size("sp")
    half = queries.shape[0] // 2
    me = lax.axis_index("sp")
    kv = from_everyone(pack_kv(key_value[:, 0, :], break_bias), "sp")
    kv = kv.reshape(blocks, -1, kv.shape[-1])
    down = [(h, blocks - 1 - h) for h in range(blocks // 2, blocks)]
    up = [(b, a) for a, b in down]
    theirs = lax.ppermute(queries[:half], "sp", down)
    tab = lax.dynamic_index_in_dim(jnp.asarray(table), me, 0, keepdims=False)
    done_rows = attend(tab, jnp.concatenate([queries, theirs], axis=0), kv, GROUP, diag_groups)
    back = lax.ppermute(done_rows[2 * half :], "sp", up)
    given = jnp.asarray(give, jnp.int32)[jnp.minimum(me, blocks - 1 - me)] * 32
    mine = (me < blocks // 2) | (jnp.arange(half)[:, None] >= given)
    attended = jnp.concatenate(
        [jnp.where(mine, done_rows[:half], back), done_rows[half : 2 * half]], axis=0
    )
    token_heads = lax.all_to_all(attended, "tp", split_axis=0, concat_axis=1, tiled=True)
    mixed = jnp.dot(token_heads, out_proj, preferred_element_type=jnp.float32)
    resid = (stream.astype(jnp.float32) + mixed).astype(jnp.bfloat16)
    wide = resid.astype(jnp.float32)
    factor = lax.rsqrt(jnp.mean(wide * wide, axis=-1, keepdims=True) + 1e-06)
    normed = (wide * factor * ffn_gain).astype(jnp.bfloat16)
    gates = 2.5 * route_score / jnp.sum(route_score, axis=1, keepdims=True)
    row_count = resid.shape[0]
    top_count = routes.shape[1]
    shard_sp = lax.axis_size("sp")
    shard_tp = lax.axis_size("tp")
    expert_count = shard_sp * shard_tp
    capacity = 2 * row_count * top_count // expert_count
    width = resid.shape[1]
    flat_expert = routes.reshape(-1)
    onehot = (flat_expert[:, None] == jnp.arange(expert_count, dtype=jnp.int32)[None, :]).astype(
        jnp.int32
    )
    rank = jnp.sum((jnp.cumsum(onehot, axis=0) - onehot) * onehot, axis=1)
    slot_ids = (flat_expert * capacity + rank).reshape(row_count, top_count)
    slot_grid = jnp.arange(expert_count * capacity, dtype=jnp.int32)
    pick = jnp.any(slot_ids[:, :, None] == slot_grid[None, None, :], axis=1).astype(jnp.bfloat16)
    outgoing = jnp.einsum("rs,rd->sd", pick, normed, preferred_element_type=jnp.float32).astype(
        jnp.bfloat16
    )
    outgoing = outgoing.reshape(expert_count, capacity, width)
    done = expert_rows(
        lax.all_to_all(outgoing, ("sp", "tp"), split_axis=0, concat_axis=0, tiled=True),
        expert_gate[0],
        expert_up[0],
        expert_down[0],
    )
    returned = lax.all_to_all(done, ("sp", "tp"), split_axis=0, concat_axis=0, tiled=True)
    flat_back = returned.reshape(expert_count * capacity, width)
    picked_rows = flat_back[slot_ids.reshape(-1)].reshape(row_count, top_count, width)
    routed = jnp.einsum("rk,rkd->rd", gates, picked_rows.astype(jnp.float32))
    shared_inner = (
        jax.nn.silu(jnp.dot(normed, shared_gate, preferred_element_type=jnp.float32))
        * jnp.dot(normed, shared_up, preferred_element_type=jnp.float32)
    ).astype(jnp.bfloat16)
    shared_out = jnp.dot(shared_inner, shared_down, preferred_element_type=jnp.float32)
    return (wide + shared_out + routed).astype(jnp.bfloat16)


def solution(mesh):
    return jax.shard_map(
        body,
        mesh=mesh,
        in_specs=(
            P("sp", "tp"),
            P("sp", "tp", None),
            P("sp", "tp"),
            P(("sp", "tp"), None),
            P(),
            P(),
            P(("sp", "tp"), None),
            P(("sp", "tp"), None),
            P(("sp", "tp"), None, None),
            P(("sp", "tp"), None, None),
            P(("sp", "tp"), None, None),
            P(),
            P(),
            P(),
        ),
        out_specs=P(("sp", "tp"), None),
        check_vma=False,
    )
```

profile of v0, /device:TPU:1, one launch (start us, length us, event | category | flops | bytes accessed | tf_op | source)
XLA Modules:
  0.0 228.5 jit_solution(13101600071419189445)
XLA Ops:
  0.0 1.0 fusion.43
  1.0 0.9 copy.53
  1.9 0.9 maximum_maximum_fusion
  2.8 1.6 broadcast_in_dim.11
  4.3 9.8 %all-to-all-start = ((bf16[32,144,256]{2,1,0:T(8,128)(2,1)}), bf16[32,144,256]{2,1,0:T(8,128)(2,1)}, u32[]{:S(2)}, u32[]{:S(2)}) async-start(bf16[32,144,256]{2,1,0:T(8,128)(2,1)} %broadcast_in_dim.11), calls=%async_computation | async-start | bytes 4718592 | tf_op jit(solution)/shard_map/all_to_all | solution.py:148
  14.2 1.4 collective-permute-start
  16.3 0.7 dynamic-slice_reduce_fusion.tab
  17.1 30.9 %collective-permute-done = bf16[128,512]{1,0:T(8,128)(2,1)S(1)} collective-permute-done((bf16[128,512]{1,0:T(8,128)(2,1)S(1)}, bf16[128,512]{1,0:T(8,128)(2,1)S(1)}, u32[]{:S(2)}, u32[]{:S(2)}) %collective-permute-start) | collective-permute-done | bytes 131104 | tf_op jit(solution)/shard_map/ppermute | solution.py:184
  48.0 41.1 %attend.1 = bf16[384,512]{1,0:T(8,128)(2,1)S(1)} custom-call(s32[322]{0:T(512)S(1)} %dynamic-slice_reduce_fusion.tab, bf16[384,512]{1,0:T(8,128)(2,1)S(1)} %pad_maximum_fusion.q_ref, bf16[32,144,256]{2,1,0:T(8,128)(2,1)} %all-to-all-done.kv_ref, bf16[256,384]{1,0:T(8,128)(2,1)S(1)} %copy-done.1), custom_call_target="tpu_custom_call" | custom-call | tf_op jit(solution)/shard_map/attend/pallas_call | solution.py:126
  89.2 2.1 collective-permute-start.1
  91.6 0.6 dynamic_slice.7
  92.8 0.5 collective-permute-done.1
  93.3 1.0 slice_select_fusion
  94.3 0.7 pad_maximum_fusion.1
  95.0 4.0 %all-to-all-start.1 = ((bf16[4,64,512]{2,1,0:T(8,128)(2,1)}), bf16[4,64,512]{2,1,0:T(8,128)(2,1)S(1)}, u32[]{:S(2)}, u32[]{:S(2)}) async-start(bf16[4,64,512]{2,1,0:T(8,128)(2,1)} %bitcast.4), calls=%async_computation.1 | async-start | bytes 524288 | tf_op jit(solution)/shard_map/all_to_all | solution.py:193
  99.3 5.3 %all-to-all-done.1 = bf16[4,64,512]{2,1,0:T(8,128)(2,1)S(1)} async-done(((bf16[4,64,512]{2,1,0:T(8,128)(2,1)}), bf16[4,64,512]{2,1,0:T(8,128)(2,1)S(1)}, u32[]{:S(2)}, u32[]{:S(2)}) %all-to-all-start.1) | async-done | bytes 262176 | tf_op jit(solution)/shard_map/all_to_all | solution.py:193
  104.6 5.1 %multiply_reduce_fusion = (f32[64]{0:T(128)S(1)}, f32[64,2048]{1,0:T(8,128)S(1)}) fusion(bf16[64,2048]{1,0:T(8,128)(2,1)S(1)} %bitcast.54, bf16[2048,2048]{1,0:T(8,128)(2,1)} %param.21, bf16[64,2048]{1,0:T(8,128)(2,1)S(1)} %copy-done.4), kind=kOutput, calls=%fused_computation.23 | convolution fusion | flops 537657280 | bytes 9437440 | tf_op jit(solution)/shard_map/dot_general | solution.py:194
  109.7 2.1 convolution_convert_fusion.1
  111.8 4.1 %reshape.84 = bf16[128,4,2048]{2,1,0:T(4,128)(2,1)} reshape(bf16[512,2048]{1,0:T(8,128)(2,1)} %convolution_convert_fusion.1) | data formatting | bytes 4194304 | tf_op jit(solution)/shard_map/reshape | solution.py:218
  115.9 43.0 %all_to_all.34 = bf16[128,4,2048]{2,1,0:T(4,128)(2,1)S(1)} all-to-all(bf16[128,4,2048]{2,1,0:T(4,128)(2,1)} %reshape.84), channel_id=1, replica_groups=mesh['sp'=32,'tp'=4] {'sp','tp'}, dimensions={0} | all-to-all | bytes 4194304 | tf_op jit(solution)/shard_map/all_to_all | solution.py:220
  159.0 1.3 copy-done.2
  160.3 3.4 %fusion.7 = f32[128,4,512]{2,0,1:T(8,128)} fusion(bf16[1,2048,512]{2,1,0:T(8,128)(2,1)S(1)} %copy-done.8, bf16[128,4,2048]{2,1,0:T(4,128)(2,1)S(1)} %all_to_all.34), kind=kOutput, calls=%fused_computation.12 | convolution fusion | flops 1073741824 | bytes 5242880 | tf_op jit(solution)/shard_map/snd,df->snf/dot_general | solution.py:152
  163.6 7.5 %convolution_convert_fusion = bf16[128,4,2048]{2,0,1:T(8,128)(2,1)} fusion(bf16[1,512,2048]{2,1,0:T(8,128)(2,1)S(1)} %copy-done, bf16[1,2048,512]{2,1,0:T(8,128)(2,1)} %param.26, bf16[128,4,2048]{2,1,0:T(4,128)(2,1)} %copy-done.2, f32[128,4,512]{2,0,1:T(8,128)} %fusion.7), kind=kOutput, calls=%fused_computation.1 | convolution fusion | flops 2150105088 | bytes 9437184 | tf_op jit(solution)/shard_map/snf,fd->snd/dot_general | solution.py:155
  171.2 4.5 %copy.50 = bf16[128,4,2048]{2,1,0:T(4,128)(2,1)} copy(bf16[128,4,2048]{2,0,1:T(8,128)(2,1)} %convolution_convert_fusion) | data formatting | bytes 4194304 | tf_op jit(solution)/shard_map/convert_element_type | solution.py:155
  175.7 5.1 %all-to-all-start.3 = ((bf16[128,4,2048]{2,1,0:T(4,128)(2,1)}), bf16[128,4,2048]{2,1,0:T(4,128)(2,1)}, u32[]{:S(2)}, u32[]{:S(2)}) async-start(bf16[128,4,2048]{2,1,0:T(4,128)(2,1)} %copy.50), calls=%async_computation.3 | async-start | bytes 4194304 | tf_op jit(solution)/shard_map/all_to_all | solution.py:225
  181.0 2.1 fusion.42
  183.2 28.0 %all-to-all-done.3 = bf16[128,4,2048]{2,1,0:T(4,128)(2,1)} async-done(((bf16[128,4,2048]{2,1,0:T(4,128)(2,1)}), bf16[128,4,2048]{2,1,0:T(4,128)(2,1)}, u32[]{:S(2)}, u32[]{:S(2)}) %all-to-all-start.3) | async-done | bytes 2097184 | tf_op jit(solution)/shard_map/all_to_all | solution.py:225
  211.2 3.9 %reshape.85 = bf16[512,2048]{1,0:T(8,128)(2,1)} reshape(bf16[128,4,2048]{2,1,0:T(4,128)(2,1)} %all-to-all-done.3) | data formatting | bytes 4194304 | tf_op jit(solution)/shard_map/reshape | solution.py:226
  215.2 5.2 %gather_fusion = bf16[256,2048]{1,0:T(8,128)(2,1)} fusion(bf16[512,2048]{1,0:T(8,128)(2,1)} %reshape.85, s32[1024]{0:T(1024)S(1)} %pad_clamp_fusion), kind=kCustom, calls=%fused_computation | custom fusion | bytes 2098176 | tf_op jit(solution)/shard_map/gather | solution.py:227
  220.4 2.3 reshape.86
  222.6 1.9 fusion.44
  224.5 4.0 %fusion.1 = bf16[64,2048]{1,0:T(8,128)(2,1)} fusion(f32[64,2048]{1,0:T(8,128)S(1)} %get-tuple-element.14, bf16[512,2048]{1,0:T(8,128)(2,1)} %param.30, bf16[2048,512]{1,0:T(8,128)(2,1)} %param.29, f32[64,1,2048]{2,1,0:T(1,128)S(1)} %fusion.44, f32[64,512]{1,0:T(8,128)S(1)} %fusion.42, f32[2048]{0:T(1024)S(1)} %copy-done.5, f32[64]{0:T(128)S(1)} %add_rsqrt_fusion), kind=kOutput, calls=%fused_computation.6 | convolution fusion | flops 269418496 | bytes 5644544 | tf_op jit(solution)/shard_map/dot_general | solution.py:233
  (48 shorter events, 1.6 us)
Async XLA Ops:
  0.0 163.6 %copy-start = (bf16[1,512,2048]{2,1,0:T(8,128)(2,1)S(1)}, bf16[1,512,2048]{2,1,0:T(8,128)(2,1)}, u32[]{:S(2)}) copy-start(bf16[1,512,2048]{2,1,0:T(8,128)(2,1)} %param.27) | copy-start | bytes 6291460
  4.3 9.8 %copy-start.3 = (bf16[256,512]{1,0:T(8,128)(2,1)S(1)}, bf16[256,512]{1,0:T(8,128)(2,1)}, u32[]{:S(2)}) copy-start(bf16[256,512]{1,0:T(8,128)(2,1)} %param.17) | copy-start | bytes 786436
  4.3 11.3 %copy-start.7 = (s32[64,4]{0,1:T(4,128)S(1)}, s32[64,4]{0,1:T(4,128)}, u32[]{:S(2)}) copy-start(s32[64,4]{0,1:T(4,128)} %param.23) | copy-start | bytes 3076
  4.3 43.7 %all-to-all-start = ((bf16[32,144,256]{2,1,0:T(8,128)(2,1)}), bf16[32,144,256]{2,1,0:T(8,128)(2,1)}, u32[]{:S(2)}, u32[]{:S(2)}) async-start(bf16[32,144,256]{2,1,0:T(8,128)(2,1)} %broadcast_in_dim.11), calls=%async_computation | async-start | bytes 4718592 | tf_op jit(solution)/shard_map/all_to_all | solution.py:148
  14.1 33.9 %copy-start.1 = (bf16[256,384]{1,0:T(8,128)(2,1)S(1)}, bf16[256,384]{1,0:T(8,128)(2,1)}, u32[]{:S(2)}) copy-start(bf16[256,384]{1,0:T(8,128)(2,1)} %constant.52.clone.tri_ref) | copy-start | bytes 589828
  14.2 33.8 %collective-permute-start = (bf16[128,512]{1,0:T(8,128)(2,1)S(1)}, bf16[128,512]{1,0:T(8,128)(2,1)S(1)}, u32[]{:S(2)}, u32[]{:S(2)}) collective-permute-start(bf16[128,512]{1,0:T(8,128)(2,1)S(1)} %slice.38), channel_id=1, source_target_pairs={{64,60},{68,56},{72,52},{76,48},{80,44},{84,40},{88,36},{92,32},{9... | collective-permute-start | bytes 393224 | tf_op jit(solution)/shard_map/ppermute | solution.py:184
  17.1 74.5 %copy-start.9 = (s32[16]{0:T(128)S(1)}, s32[16]{0:T(128)}, u32[]{:S(2)}) copy-start(s32[16]{0:T(128)} %constant.53.clone) | copy-start | bytes 196
  89.2 15.4 %copy-start.4 = (bf16[64,2048]{1,0:T(8,128)(2,1)S(1)}, bf16[64,2048]{1,0:T(8,128)(2,1)}, u32[]{:S(2)}) copy-start(bf16[64,2048]{1,0:T(8,128)(2,1)} %param.20) | copy-start | bytes 786436
  89.2 4.1 %collective-permute-start.1 = (bf16[128,512]{1,0:T(8,128)(2,1)S(1)}, bf16[128,512]{1,0:T(8,128)(2,1)}, u32[]{:S(2)}, u32[]{:S(2)}) collective-permute-start(bf16[128,512]{1,0:T(8,128)(2,1)S(1)} %slice.57), channel_id=1, source_target_pairs={{60,64},{56,68},{52,72},{48,76},{44,80},{40,84},{36,88},{32,92},{2... | collective-permute-start | bytes 393224 | tf_op jit(solution)/shard_map/ppermute | solution.py:187
  95.0 9.5 %all-to-all-start.1 = ((bf16[4,64,512]{2,1,0:T(8,128)(2,1)}), bf16[4,64,512]{2,1,0:T(8,128)(2,1)S(1)}, u32[]{:S(2)}, u32[]{:S(2)}) async-start(bf16[4,64,512]{2,1,0:T(8,128)(2,1)} %bitcast.4), calls=%async_computation.1 | async-start | bytes 524288 | tf_op jit(solution)/shard_map/all_to_all | solution.py:193
  104.6 5.1 %copy-start.5 = (f32[2048]{0:T(1024)S(1)}, f32[2048]{0:T(1024)}, u32[]{:S(2)}) copy-start(f32[2048]{0:T(1024)} %param.22) | copy-start | bytes 24580
  115.9 44.3 %copy-start.8 = (bf16[1,2048,512]{2,1,0:T(8,128)(2,1)S(1)}, bf16[1,2048,512]{2,1,0:T(8,128)(2,1)}, u32[]{:S(2)}) copy-start(bf16[1,2048,512]{2,1,0:T(8,128)(2,1)} %param.25) | copy-start | bytes 6291460
  159.0 1.3 copy-start.2
  175.7 5.2 %copy-start.6 = (f32[64,4]{0,1:T(4,128)S(1)}, f32[64,4]{0,1:T(4,128)}, u32[]{:S(2)}) copy-start(f32[64,4]{0,1:T(4,128)} %param.24) | copy-start | bytes 3076
  175.7 35.5 %all-to-all-start.3 = ((bf16[128,4,2048]{2,1,0:T(4,128)(2,1)}), bf16[128,4,2048]{2,1,0:T(4,128)(2,1)}, u32[]{:S(2)}, u32[]{:S(2)}) async-start(bf16[128,4,2048]{2,1,0:T(4,128)(2,1)} %copy.50), calls=%async_computation.3 | async-start | bytes 4194304 | tf_op jit(solution)/shard_map/all_to_all | solution.py:225
where the time goes:
time: 229 us
  waiting for transfers between devices  64.7 us (28%)
  blocking collectives  43 us (19%)
  Pallas kernels  41.1 us (18%)
  local copies, waits for them, and re-layouts  27 us (12%)
  matrix products  26.1 us (11%)
  starting transfers between devices  22.3 us (10%)
  other arithmetic  3.23 us (1%)
    all_to_all x1, blocking collectives, body(): lax.all_to_all(outgoing, ('sp', 'tp'), split_axis=0, concat_axis=0, tiled...  43 us
    pallas_call x1, Pallas kernels, attend(): pl.pallas_call(functools.partial(attend_kernel, group, ld), out_shape=jax...  41.1 us
    ppermute x1, waiting for transfers between devices, body(): theirs = lax.ppermute(queries[:half], 'sp', down)  30.9 us
    all_to_all x1, waiting for transfers between devices, body(): lax.all_to_all(done, ('sp', 'tp'), split_axis=0, concat_axis=0, tiled=True)  28 us
    all_to_all x1, starting transfers between devices, from_everyone(): return lax.all_to_all(copies, axis, split_axis=0, concat_axis=0, tiled=True)  9.77 us
    dot_general x1, matrix products, expert_rows(): jnp.einsum('snf,fd->snd', inner, w_down, preferred_element_type=jnp.float32)  7.51 us
    all_to_all x1, waiting for transfers between devices, body(): lax.all_to_all(attended, 'tp', split_axis=0, concat_axis=1, tiled=True)  5.29 us
    gather x1, local copies, waits for them, and re-layouts, body(): flat_back[slot_ids.reshape(-1)].reshape(row_count, top_count, width)  5.2 us
  transfers between devices with their start and end apart: 5, of which 4 were waited for; matrix products, arithmetic and copies ran while one was open for 2% of the time, Pallas kernels for 0%

commit v1 on v0

--- a/solution.py
+++ b/solution.py
@@ -134,104 +134,399 @@
     )(tab, q_all, kv, jnp.asarray(triangle(), jnp.bfloat16))
 
 
-def pack_kv(key_value, bias):
-    kt = key_value[:, :64].T
-    b = bias.T
-    v = key_value[:, 64:]
+MESH = pl.DeviceIdType.MESH
+VM = pl.BlockSpec(memory_space=pltpu.VMEM)
+
+
+def place():
+    sp, x = lax.axis_index("sp"), lax.axis_index("tp")
+    return sp // 8, (sp // 2) % 4, sp % 2, x
+
+
+def given_tiles(sp, thresholds):
+    low = jnp.minimum(sp, 31 - sp)
+    n = jnp.int32(0)
+    for t in thresholds:
+        n = n + jnp.where(low < t, 1, 0)
+    return n
+
+
+def pack_kernel(kv_ref, bias_ref, out_ref):
+    f32, bf16 = jnp.float32, jnp.bfloat16
+    kv = kv_ref[...].astype(f32)
+    keys = kv.T[0:64].astype(bf16)
+    shift = jnp.concatenate([bias_ref[...].astype(f32), jnp.zeros((256, 120), f32)], axis=1).T[0:8]
+    shifts = jnp.concatenate([shift, shift], axis=0).astype(bf16)
+    v = kv[:, 64:]
     left = jnp.concatenate([v[0:64], v[128:192]], axis=1)
     right = jnp.concatenate([v[64:128], v[192:256]], axis=1)
-    return jnp.concatenate([kt, b, b, jnp.concatenate([left, right], axis=1)], axis=0)
-
-
-def from_everyone(array, axis):
-    copies = jnp.broadcast_to(array, (lax.axis_size(axis), *array.shape))
-    return lax.all_to_all(copies, axis, split_axis=0, concat_axis=0, tiled=True)
-
-
-def expert_rows(arrived, w_gate, w_up, w_down):
-    gate_part = jnp.einsum("snd,df->snf", arrived, w_gate, preferred_element_type=jnp.float32)
-    up_part = jnp.einsum("snd,df->snf", arrived, w_up, preferred_element_type=jnp.float32)
-    inner = (jax.nn.silu(gate_part) * up_part).astype(jnp.bfloat16)
-    return jnp.einsum("snf,fd->snd", inner, w_down, preferred_element_type=jnp.float32).astype(
-        jnp.bfloat16
+    out_ref[0:64, :] = keys
+    out_ref[64:80, :] = shifts
+    out_ref[80:144, :] = jnp.concatenate([left, right], axis=1).astype(bf16)
+
+
+def pack(key_value, bias):
+    return pl.pallas_call(
+        pack_kernel,
+        out_shape=jax.ShapeDtypeStruct((144, 256), jnp.bfloat16),
+        in_specs=[VM, VM],
+        out_specs=VM,
+        name="pack",
+    )(key_value, bias)
+
+
+def gather_kernel(mine_ref, q_ref, kv_ref, theirs_ref, send, recv_a, recv_b, recv_s, q_send, q_recv, local):
+    z, y, c, x = place()
+    sp = (z * 4 + y) * 2 + c
+
+    def at(zz, yy, cc):
+        return (zz % 4 * 4 + yy % 4) * 2 + cc
+
+    barrier = pltpu.get_barrier_semaphore()
+    for d in (1, 2, 3):
+        pl.semaphore_signal(barrier, inc=1, device_id=(at(z + d, y, c), x), device_id_type=MESH)
+        pl.semaphore_signal(barrier, inc=1, device_id=(at(z, y + d, c), x), device_id_type=MESH)
+    pl.semaphore_signal(barrier, inc=1, device_id=(at(z, y, 1 - c), x), device_id_type=MESH)
+    pl.semaphore_signal(barrier, inc=1, device_id=(31 - sp, x), device_id_type=MESH)
+    own = pltpu.make_async_copy(mine_ref, kv_ref.at[sp], local)
+    own.start()
+    pl.semaphore_wait(barrier, 8)
+    sends = []
+
+    def push(src, dst, recv, device):
+        copy = pltpu.make_async_remote_copy(
+            src_ref=src, dst_ref=dst, send_sem=send.at[len(sends)], recv_sem=recv, device_id=(device, x), device_id_type=MESH
+        )
+        copy.start()
+        sends.append(copy)
+
+    def part_a(ref, block=None):
+        return ref.at[pl.ds(0, 80), :] if block is None else ref.at[block, pl.ds(0, 80), :]
+
+    def part_b(ref, block=None):
+        return ref.at[pl.ds(80, 64), :] if block is None else ref.at[block, pl.ds(80, 64), :]
+
+    for d in (1, 3, 2):
+        push(part_a(mine_ref), part_a(kv_ref, sp), recv_a.at[d, 0], at(z + d, y, c))
+        push(part_b(mine_ref), part_b(kv_ref, sp), recv_b.at[0, d], at(z, y + d, c))
+    for d in (1, 3, 2):
+        push(part_a(mine_ref), part_a(kv_ref, sp), recv_a.at[0, d], at(z, y + d, c))
+        push(part_b(mine_ref), part_b(kv_ref, sp), recv_b.at[d, 0], at(z + d, y, c))
+    push(part_a(mine_ref), part_a(kv_ref, sp), recv_s.at[0, 0, 0], at(z, y, 1 - c))
+    push(part_b(mine_ref), part_b(kv_ref, sp), recv_s.at[0, 0, 1], at(z, y, 1 - c))
+    theirs = pltpu.make_async_remote_copy(
+        src_ref=q_ref.at[pl.ds(0, 128), :], dst_ref=theirs_ref, send_sem=q_send, recv_sem=q_recv, device_id=(31 - sp, x), device_id_type=MESH
     )
 
+    @pl.when(sp >= 16)
+    def _():
+        theirs.start()
+
+    def landed(dz, dy, which):
+        block = at(z - dz, y - dy, c)
+        ref = part_a(kv_ref, block) if which == 0 else part_b(kv_ref, block)
+        sem = (recv_a if which == 0 else recv_b).at[dz, dy]
+        pltpu.make_async_copy(ref, ref, sem).wait()
+        return ref
+
+    for d in (1, 3, 2):
+        ref = landed(d, 0, 0)
+        for e in (1, 3, 2):
+            push(ref, ref, recv_a.at[d, e], at(z, y + e, c))
+        push(ref, ref, recv_s.at[d, 0, 0], at(z, y, 1 - c))
+        ref = landed(0, d, 1)
+        for e in (1, 3, 2):
+            push(ref, ref, recv_b.at[e, d], at(z + e, y, c))
+        push(ref, ref, recv_s.at[0, d, 1], at(z, y, 1 - c))
+    for d in (1, 3, 2):
+        ref = landed(0, d, 0)
+        push(ref, ref, recv_s.at[0, d, 0], at(z, y, 1 - c))
+        ref = landed(d, 0, 1)
+        push(ref, ref, recv_s.at[d, 0, 1], at(z, y, 1 - c))
+    for d in (1, 3, 2):
+        for e in (1, 3, 2):
+            ref = landed(d, e, 0)
+            push(ref, ref, recv_s.at[d, e, 0], at(z, y, 1 - c))
+            ref = landed(e, d, 1)
+            push(ref, ref, recv_s.at[e, d, 1], at(z, y, 1 - c))
+    for dz in range(4):
+        for dy in range(4):
+            block = at(z - dz, y - dy, 1 - c)
+            for which in (0, 1):
+                ref = part_a(kv_ref, block) if which == 0 else part_b(kv_ref, block)
+                pltpu.make_async_copy(ref, ref, recv_s.at[dz, dy, which]).wait()
+    own.wait()
+    for copy in sends:
+        copy.wait_send()
+
+    @pl.when(sp >= 16)
+    def _():
+        theirs.wait_send()
+
+    @pl.when(sp < 16)
+    def _():
+        theirs.wait_recv()
+
+
+def gather(mine, queries):
+    return pl.pallas_call(
+        gather_kernel,
+        out_shape=(jax.ShapeDtypeStruct((32, 144, 256), jnp.bfloat16), jax.ShapeDtypeStruct((128, 512), jnp.bfloat16)),
+        in_specs=[VM, VM],
+        out_specs=(VM, VM),
+        scratch_shapes=[
+            pltpu.SemaphoreType.DMA((64,)),
+            pltpu.SemaphoreType.DMA((4, 4)),
+            pltpu.SemaphoreType.DMA((4, 4)),
+            pltpu.SemaphoreType.DMA((4, 4, 2)),
+            pltpu.SemaphoreType.DMA,
+            pltpu.SemaphoreType.DMA,
+            pltpu.SemaphoreType.DMA,
+        ],
+        compiler_params=pltpu.CompilerParams(collective_id=0, has_side_effects=True),
+        name="gather",
+    )(mine, queries)
+
+
+def swap_kernel(thresholds, att_ref, out_ref, send, recv):
+    z, y, c, x = place()
+    sp = (z * 4 + y) * 2 + c
+    other = 31 - sp
+    n = given_tiles(sp, thresholds)
+    low = sp < 16
+    barrier = pltpu.get_barrier_semaphore()
+    for d in (1, 2, 3):
+        pl.semaphore_signal(barrier, inc=1, device_id=(sp, (x + d) % 4), device_id_type=MESH)
+    for d in range(4):
+        pl.semaphore_signal(barrier, inc=1, device_id=(other, (x + d) % 4), device_id_type=MESH)
+    pl.semaphore_wait(barrier, 7)
+
+    def tile(s):
+        return att_ref.at[pl.ds(s * 32, 32), :]
+
+    def spot(t, half):
+        return out_ref.at[t, pl.ds(half * 32, 32), :]
+
+    jobs = []
+    for d in (1, 3, 2, 0):
+        for half in (0, 1):
+            s = (x + d) % 4 * 2 + half
+            made = jnp.logical_or(low, s >= n)
+            if d == 0:
+                copy = pltpu.make_async_copy(tile(s), spot(x, half), recv.at[x * 2 + half])
+            else:
+                copy = pltpu.make_async_remote_copy(
+                    src_ref=tile(s), dst_ref=spot(x, half), send_sem=send.at[d * 2 + half], recv_sem=recv.at[x * 2 + half],
+                    device_id=(sp, (x + d) % 4), device_id_type=MESH,
+                )
+            jobs.append((made, copy, d != 0))
+    for s in range(len(thresholds)):
+        made = jnp.logical_and(low, s < n)
+        copy = pltpu.make_async_remote_copy(
+            src_ref=tile(8 + s), dst_ref=spot(x, s % 2), send_sem=send.at[8 + s], recv_sem=recv.at[x * 2 + s % 2],
+            device_id=(other, s // 2), device_id_type=MESH,
+        )
+        jobs.append((made, copy, True))
+    for made, copy, _ in jobs:
+        pl.when(made)(copy.start)
+    for t in range(4):
+        for half in (0, 1):
+            pltpu.make_async_copy(spot(t, half), spot(t, half), recv.at[t * 2 + half]).wait()
+    for made, copy, remote in jobs:
+        if remote:
+            pl.when(made)(copy.wait_send)
+
+
+def swap(att, thresholds):
+    return pl.pallas_call(
+        functools.partial(swap_kernel, thresholds),
+        out_shape=jax.ShapeDtypeStruct((4, 64, 512), jnp.bfloat16),
+        in_specs=[VM],
+        out_specs=VM,
+        scratch_shapes=[pltpu.SemaphoreType.DMA((12,)), pltpu.SemaphoreType.DMA((8,))],
+        compiler_params=pltpu.CompilerParams(collective_id=1, has_side_effects=True),
+        name="swap",
+    )(att)
+
+
+def offsets():
+    every = [(dz, dy, dx, dc) for dz in range(4) for dy in range(4) for dx in range(4) for dc in range(2)][1:]
+    order = np.random.default_rng(1).permutation(len(every))
+    return [every[k] for k in order]
+
+
+def exchange_kernel(x_ref, o_ref, send, recv, local):
+    z, y, c, x = place()
+    me = ((z * 4 + y) * 2 + c) * 4 + x
+
+    def peer(o):
+        return (((z + o[0]) % 4 * 4 + (y + o[1]) % 4) * 2 + (c + o[3]) % 2, (x + o[2]) % 4)
+
+    steps = offsets()
+    barrier = pltpu.get_barrier_semaphore()
+    for o in steps:
+        pl.semaphore_signal(barrier, inc=1, device_id=peer(o), device_id_type=MESH)
+    own = pltpu.make_async_copy(x_ref.at[me], o_ref.at[me], local)
+    own.start()
+    pl.semaphore_wait(barrier, len(steps))
+    for o in steps:
+        s, t = peer(o)
+        pltpu.make_async_remote_copy(
+            src_ref=x_ref.at[s * 4 + t], dst_ref=o_ref.at[me], send_sem=send, recv_sem=recv, device_id=(s, t), device_id_type=MESH
+        ).start()
+    own.wait()
+    count = len(steps)
+    pltpu.make_async_copy(x_ref.at[pl.ds(0, count)], o_ref.at[pl.ds(0, count)], send).wait()
+    pltpu.make_async_copy(x_ref.at[pl.ds(0, count)], o_ref.at[pl.ds(0, count)], recv).wait()
+
+
+def exchange(x, number):
+    return pl.pallas_call(
+        exchange_kernel,
+        out_shape=jax.ShapeDtypeStruct(x.shape, x.dtype),
+        in_specs=[VM],
+        out_specs=VM,
+        scratch_shapes=[pltpu.SemaphoreType.DMA] * 3,
+        compiler_params=pltpu.CompilerParams(collective_id=number, has_side_effects=True, vmem_limit_bytes=32 * 1024 * 1024),
+        name="exchange",
+    )(x)
+
+
+def slot_codes(shape, dim):
+    at = lax.broadcasted_iota(jnp.int32, shape, dim)
+    return at // 8, at // 4 % 2, at % 4
+
+
+def project_kernel(th_ref, w_ref, stream_ref, gain_ref, routes_ref, sg_ref, su_ref, sd_ref, out_ref, base_ref):
+    f32, bf16 = jnp.float32, jnp.bfloat16
+    dot = functools.partial(jnp.dot, preferred_element_type=f32)
+    mixed = sum(dot(th_ref[t], w_ref[pl.ds(512 * t, 512), :]) for t in range(4))
+    resid = (stream_ref[...].astype(f32) + mixed).astype(bf16).astype(f32)
+    factor = lax.rsqrt(jnp.mean(resid * resid, axis=1, keepdims=True) + 1e-06)
+    normed = (resid * factor * gain_ref[...]).astype(bf16)
+    expert = lax.broadcasted_iota(jnp.int32, (128, 64), 0)
+    named = jnp.zeros((128, 64), f32)
+    for k in range(4):
+        named = jnp.where(routes_ref[pl.ds(k, 1), :] == expert, 1.0, named)
+    earlier = lax.broadcasted_iota(jnp.int32, (64, 64), 0) < lax.broadcasted_iota(jnp.int32, (64, 64), 1)
+    rank = dot(named.astype(bf16), earlier.astype(f32).astype(bf16))
+    e, h, k = slot_codes((1024, 128), 0)
+    spread = (e == lax.broadcasted_iota(jnp.int32, (1024, 128), 1)).astype(f32).astype(bf16)
+    both = dot(spread, jnp.concatenate([named, rank], axis=1).astype(bf16))
+    _, h, k = slot_codes((1024, 64), 0)
+    taken = jnp.where(both[:, 64:] == k.astype(f32), both[:, :64], 0.0)
+    pick = jnp.concatenate([jnp.where(h == 0, taken, 0.0), jnp.where(h == 1, taken, 0.0)], axis=1).astype(bf16)
+    out_ref[...] = dot(pick, jnp.concatenate([normed[:, :1024], normed[:, 1024:]], axis=0)).astype(bf16)
+    gate = dot(normed, sg_ref[...])
+    inner = (gate * jax.nn.sigmoid(gate) * dot(normed, su_ref[...])).astype(bf16)
+    base_ref[...] = resid + dot(inner, sd_ref[...])
+
+
+def project(th, w, stream, gain, routes_t, sg, su, sd):
+    return pl.pallas_call(
+        project_kernel,
+        out_shape=(jax.ShapeDtypeStruct((1024, 1024), jnp.bfloat16), jax.ShapeDtypeStruct((64, 2048), jnp.float32)),
+        in_specs=[VM] * 8,
+        out_specs=(VM, VM),
+        compiler_params=pltpu.CompilerParams(vmem_limit_bytes=48 * 1024 * 1024),
+        name="project",
+    )(th, w, stream, gain, routes_t, sg, su, sd)
+
+
+def expert_kernel(x_ref, g_ref, u_ref, d_ref, out_ref):
+    f32, bf16 = jnp.float32, jnp.bfloat16
+    dot = functools.partial(jnp.dot, preferred_element_type=f32)
+    top = lax.broadcasted_iota(jnp.int32, (16, 8, 1024), 1) < 4
+
+    def some(j, _):
+        rows = pl.ds(j * 256, 256)
+        wide = x_ref[rows, :].astype(f32).reshape(16, 2, 8, 1024)
+        a, b = wide[:, 0], wide[:, 1]
+        left = jnp.where(top, a, pltpu.roll(b, 4, 1)).reshape(128, 1024).astype(bf16)
+        right = jnp.where(top, pltpu.roll(a, 4, 1), b).reshape(128, 1024).astype(bf16)
+        gate = dot(left, g_ref[0:1024, :]) + dot(right, g_ref[1024:2048, :])
+        up = dot(left, u_ref[0:1024, :]) + dot(right, u_ref[1024:2048, :])
+        inner = (gate * jax.nn.sigmoid(gate) * up).astype(bf16)
+        lo = dot(inner, d_ref[:, 0:1024]).reshape(16, 8, 1024)
+        hi = dot(inner, d_ref[:, 1024:2048]).reshape(16, 8, 1024)
+        first = jnp.where(top, lo, pltpu.roll(hi, 4, 1))
+        second = jnp.where(top, pltpu.roll(lo, 4, 1), hi)
+        out_ref[rows, :] = jnp.stack([first, second], axis=1).reshape(256, 1024).astype(bf16)
+        return 0
+
+    lax.fori_loop(0, 4, some, 0)
+
+
+def experts(x, g, u, d):
+    return pl.pallas_call(
+        expert_kernel,
+        out_shape=jax.ShapeDtypeStruct((1024, 1024), jnp.bfloat16),
+        in_specs=[VM] * 4,
+        out_specs=VM,
+        compiler_params=pltpu.CompilerParams(vmem_limit_bytes=48 * 1024 * 1024),
+        name="experts",
+    )(x, g, u, d)
+
+
+def combine_kernel(back_ref, base_ref, routes_ref, score_ref, out_ref):
+    f32, bf16 = jnp.float32, jnp.bfloat16
+    dot = functools.partial(jnp.dot, preferred_element_type=f32)
+    score = score_ref[...]
+    gates = 2.5 * score / jnp.sum(score, axis=1, keepdims=True)
+    expert = lax.broadcasted_iota(jnp.int32, (64, 128), 1)
+    named = jnp.zeros((64, 128), f32)
+    gate = jnp.zeros((64, 128), f32)
+    for k in range(4):
+        hit = routes_ref[:, k : k + 1] == expert
+        named = jnp.where(hit, 1.0, named)
+        gate = jnp.where(hit, gates[:, k : k + 1], gate)
+    earlier = lax.broadcasted_iota(jnp.int32, (64, 64), 1) < lax.broadcasted_iota(jnp.int32, (64, 64), 0)
+    rank = dot(earlier.astype(f32).astype(bf16), named.astype(bf16))
+    high = gate.astype(bf16)
+    low = (gate - high.astype(f32)).astype(bf16)
+    e, _, _ = slot_codes((128, 1024), 1)
+    spread = (e == lax.broadcasted_iota(jnp.int32, (128, 1024), 0)).astype(f32).astype(bf16)
+    wide = dot(jnp.concatenate([rank.astype(bf16), high, low], axis=0), spread)
+    _, h, k = slot_codes((64, 1024), 1)
+    mine = wide[0:64] == k.astype(f32)
+    parts = []
+    for half in (0, 1):
+        for piece in (wide[64:128], wide[128:192]):
+            parts.append(jnp.where(mine & (h == half), piece, 0.0))
+    total = dot(jnp.concatenate(parts, axis=0).astype(bf16), back_ref[...])
+    base = base_ref[...]
+    out_ref[:, 0:1024] = (base[:, 0:1024] + total[0:64] + total[64:128]).astype(bf16)
+    out_ref[:, 1024:2048] = (base[:, 1024:2048] + total[128:192] + total[192:256]).astype(bf16)
+
+
+def combine(back, base, routes, score):
+    return pl.pallas_call(
+        combine_kernel,
+        out_shape=jax.ShapeDtypeStruct((64, 2048), jnp.bfloat16),
+        in_specs=[VM] * 4,
+        out_specs=VM,
+        compiler_params=pltpu.CompilerParams(vmem_limit_bytes=32 * 1024 * 1024),
+        name="combine",
+    )(back, base, routes, score)
+
 
 def body(
-    queries,
-    key_value,
-    break_bias,
-    stream,
-    out_proj,
-    ffn_gain,
-    routes,
-    route_score,
-    expert_gate,
-    expert_up,
-    expert_down,
-    shared_gate,
-    shared_up,
-    shared_down,
+    queries, key_value, break_bias, stream, out_proj, ffn_gain, routes, route_score,
+    expert_gate, expert_up, expert_down, shared_gate, shared_up, shared_down,
 ):
     table, give, diag_groups, _ = schedule(lax.axis_size("sp"), queries.shape[0] // 32, GROUP)
-    blocks = lax.axis_size("sp")
-    half = queries.shape[0] // 2
-    me = lax.axis_index("sp")
-    kv = from_everyone(pack_kv(key_value[:, 0, :], break_bias), "sp")
-    kv = kv.reshape(blocks, -1, kv.shape[-1])
-    down = [(h, blocks - 1 - h) for h in range(blocks // 2, blocks)]
-    up = [(b, a) for a, b in down]
-    theirs = lax.ppermute(queries[:half], "sp", down)
-    tab = lax.dynamic_index_in_dim(jnp.asarray(table), me, 0, keepdims=False)
-    done_rows = attend(tab, jnp.concatenate([queries, theirs], axis=0), kv, GROUP, diag_groups)
-    back = lax.ppermute(done_rows[2 * half :], "sp", up)
-    given = jnp.asarray(give, jnp.int32)[jnp.minimum(me, blocks - 1 - me)] * 32
-    mine = (me < blocks // 2) | (jnp.arange(half)[:, None] >= given)
-    attended = jnp.concatenate(
-        [jnp.where(mine, done_rows[:half], back), done_rows[half : 2 * half]], axis=0
+    thresholds = tuple(int((give >= k).sum()) for k in range(1, int(give.max()) + 1))
+    kv, theirs = gather(pack(key_value[:, 0, :], break_bias), queries)
+    tab = lax.dynamic_index_in_dim(jnp.asarray(table), lax.axis_index("sp"), 0, keepdims=False)
+    made = attend(tab, jnp.concatenate([queries, theirs], axis=0), kv, GROUP, diag_groups)
+    heads = swap(made, thresholds)
+    outgoing, base = project(
+        heads, out_proj, stream, ffn_gain.reshape(1, -1), routes.T, shared_gate, shared_up, shared_down
     )
-    token_heads = lax.all_to_all(attended, "tp", split_axis=0, concat_axis=1, tiled=True)
-    mixed = jnp.dot(token_heads, out_proj, preferred_element_type=jnp.float32)
-    resid = (stream.astype(jnp.float32) + mixed).astype(jnp.bfloat16)
-    wide = resid.astype(jnp.float32)
-    factor = lax.rsqrt(jnp.mean(wide * wide, axis=-1, keepdims=True) + 1e-06)
-    normed = (wide * factor * ffn_gain).astype(jnp.bfloat16)
-    gates = 2.5 * route_score / jnp.sum(route_score, axis=1, keepdims=True)
-    row_count = resid.shape[0]
-    top_count = routes.shape[1]
-    shard_sp = lax.axis_size("sp")
-    shard_tp = lax.axis_size("tp")
-    expert_count = shard_sp * shard_tp
-    capacity = 2 * row_count * top_count // expert_count
-    width = resid.shape[1]
-    flat_expert = routes.reshape(-1)
-    onehot = (flat_expert[:, None] == jnp.arange(expert_count, dtype=jnp.int32)[None, :]).astype(
-        jnp.int32
-    )
-    rank = jnp.sum((jnp.cumsum(onehot, axis=0) - onehot) * onehot, axis=1)
-    slot_ids = (flat_expert * capacity + rank).reshape(row_count, top_count)
-    slot_grid = jnp.arange(expert_count * capacity, dtype=jnp.int32)
-    pick = jnp.any(slot_ids[:, :, None] == slot_grid[None, None, :], axis=1).astype(jnp.bfloat16)
-    outgoing = jnp.einsum("rs,rd->sd", pick, normed, preferred_element_type=jnp.float32).astype(
-        jnp.bfloat16
-    )
-    outgoing = outgoing.reshape(expert_count, capacity, width)
-    done = expert_rows(
-        lax.all_to_all(outgoing, ("sp", "tp"), split_axis=0, concat_axis=0, tiled=True),
-        expert_gate[0],
-        expert_up[0],
-        expert_down[0],
-    )
-    returned = lax.all_to_all(done, ("sp", "tp"), split_axis=0, concat_axis=0, tiled=True)
-    flat_back = returned.reshape(expert_count * capacity, width)
-    picked_rows = flat_back[slot_ids.reshape(-1)].reshape(row_count, top_count, width)
-    routed = jnp.einsum("rk,rkd->rd", gates, picked_rows.astype(jnp.float32))
-    shared_inner = (
-        jax.nn.silu(jnp.dot(normed, shared_gate, preferred_element_type=jnp.float32))
-        * jnp.dot(normed, shared_up, preferred_element_type=jnp.float32)
-    ).astype(jnp.bfloat16)
-    shared_out = jnp.dot(shared_inner, shared_down, preferred_element_type=jnp.float32)
-    return (wide + shared_out + routed).astype(jnp.bfloat16)
+    arrived = exchange(outgoing.reshape(128, 8, 1024), 2)
+    done = experts(arrived.reshape(1024, 1024), expert_gate[0], expert_up[0], expert_down[0])
+    back = exchange(done.reshape(128, 8, 1024), 3)
+    return combine(back.reshape(1024, 1024), base, routes, route_score)
 
 
 def solution(mesh):

time: 229 us -> 173 us (0.76)
  Pallas kernels: 41.1 us -> 165 us
  waiting for transfers between devices: 64.7 us -> 0 us
  blocking collectives: 43 us -> 0 us
  matrix products: 26.1 us -> 0 us
  starting transfers between devices: 22.3 us -> 0 us
  local copies, waits for them, and re-layouts: 27 us -> 6.62 us
    pallas_call x0 -> x8, Pallas kernels: none -> 123 us  [the longest x2 72.1 us: exchange(): pl.pallas_call(exchange_kernel, out_shape=jax.ShapeDtypeStruct(x.shape, x...]
    all_to_all x1 -> x0, blocking collectives: 43 us -> none  [body(): lax.all_to_all(outgoing, ('sp', 'tp'), split_axis=0, concat_axis=0, tiled...]
    all_to_all x3 -> x0, waiting for transfers between devices: 33.3 us -> none  [the longest x1 28 us: body(): lax.all_to_all(done, ('sp', 'tp'), split_axis=0, concat_axis=0, tiled=True)]
    ppermute x2 -> x0, waiting for transfers between devices: 31.4 us -> none  [the longest x1 30.9 us: body(): theirs = lax.ppermute(queries[:half], 'sp', down)]
    dot_general x7 -> x0, matrix products: 26.1 us -> none  [the longest x1 7.51 us: expert_rows(): jnp.einsum('snf,fd->snd', inner, w_down, preferred_element_type=jnp.float32)]
    all_to_all x3 -> x0, starting transfers between devices: 18.8 us -> none  [the longest x1 9.77 us: from_everyone(): return lax.all_to_all(copies, axis, split_axis=0, concat_axis=0, tiled=True)]
    reshape x3 -> x0, local copies, waits for them, and re-layouts: 10.3 us -> none  [the longest x1 4.1 us: body(): outgoing = outgoing.reshape(expert_count, capacity, width)]
    gather x1 -> x0, local copies, waits for them, and re-layouts: 5.2 us -> none  [body(): flat_back[slot_ids.reshape(-1)].reshape(row_count, top_count, width)]
  transfers between devices with their start and end apart: 5 -> 0, of which waited for: 4 -> 0; matrix products, arithmetic and copies ran while one was open for 2% -> 0% of each run, Pallas kernels for 0% -> 0%
where the time goes in v1:
time: 173 us; the launch traced here: 172 us
  Pallas kernels  165 us (95%)
  local copies, waits for them, and re-layouts  6.62 us (4%)
    pallas_call x2, Pallas kernels, exchange(): pl.pallas_call(exchange_kernel, out_shape=jax.ShapeDtypeStruct(x.shape, x...  72.1 us
    pallas_call x1, Pallas kernels, attend(): pl.pallas_call(functools.partial(attend_kernel, group, ld), out_shape=jax...  41 us
    pallas_call x1, Pallas kernels, gather(): pl.pallas_call(gather_kernel, out_shape=(jax.ShapeDtypeStruct((32, 144, 2...  24 us
    pallas_call x1, Pallas kernels, project(): pl.pallas_call(project_kernel, out_shape=(jax.ShapeDtypeStruct((1024, 102...  8.61 us
    pallas_call x1, Pallas kernels, swap(): pl.pallas_call(functools.partial(swap_kernel, thresholds), out_shape=jax....  8 us
    pallas_call x1, Pallas kernels, experts(): pl.pallas_call(expert_kernel, out_shape=jax.ShapeDtypeStruct((1024, 1024)...  7.36 us
    unnamed x21, local copies, waits for them, and re-layouts  5.89 us

profile of v1, /device:TPU:1, one launch (start us, length us, event | category | flops | bytes accessed | tf_op | source)
XLA Modules:
  0.0 172.3 jit_solution(18079844263505198583)
XLA Ops:
  0.0 0.7 dynamic-slice_reduce_fusion.tab
  0.7 1.4 copy.17.bias_ref
  2.1 1.6 pack.1.mine_ref
  3.8 24.0 %gather.1 = (bf16[32,144,256]{2,1,0:T(8,128)(2,1)}, bf16[128,512]{1,0:T(8,128)(2,1)}) custom-call(bf16[144,256]{1,0:T(8,128)(2,1)} %pack.1.mine_ref, bf16[256,512]{1,0:T(8,128)(2,1)} %q_ref.1), custom_call_target="tpu_custom_call" | custom-call | tf_op jit(solution)/shard_map/gather/pallas_call | solution.py:272
  27.8 1.0 pad_maximum_fusion.q_ref
  28.8 0.0 copy-start
  28.8 1.7 copy-done
  30.5 0.0 copy-start.5
  30.5 0.9 copy-done.5
  31.4 0.0 copy-start.1
  31.4 0.0 copy-start.4
  31.4 0.0 copy-start.6
  31.4 0.0 copy-start.7
  31.4 41.0 %attend.1.att_ref = bf16[384,512]{1,0:T(8,128)(2,1)S(1)} custom-call(s32[322]{0:T(512)S(1)} %dynamic-slice_reduce_fusion.tab, bf16[384,512]{1,0:T(8,128)(2,1)S(1)} %pad_maximum_fusion.q_ref, bf16[32,144,256]{2,1,0:T(8,128)(2,1)S(1)} %copy-done, bf16[256,384]{1,0:T(8,128)(2,1)S(1)} %copy-done.5), custom_call_target="tpu_custom_call" | custom-call | tf_op jit(solution)/shard_map/attend/pallas_call | solution.py:126
  72.5 0.0 copy-start.2
  72.5 0.7 copy-done.2
  73.2 8.0 %swap.1.th_ref = bf16[4,64,512]{2,1,0:T(8,128)(2,1)} custom-call(bf16[384,512]{1,0:T(8,128)(2,1)} %copy-done.2), custom_call_target="tpu_custom_call" | custom-call | tf_op jit(solution)/shard_map/swap/pallas_call | solution.py:341
  81.2 0.0 copy-done.1
  81.2 0.0 copy-done.4
  81.2 0.0 copy-done.6
  81.2 0.0 copy-done.7
  81.3 0.0 copy-start.3
  81.3 0.9 copy-done.3
  82.2 8.6 %project.1 = (bf16[1024,1024]{1,0:T(8,128)(2,1)S(1)}, f32[64,2048]{1,0:T(8,128)S(1)}) custom-call(bf16[4,64,512]{2,1,0:T(8,128)(2,1)S(1)} %copy-done.3, bf16[2048,2048]{1,0:T(8,128)(2,1)} %w_ref.1, bf16[64,2048]{1,0:T(8,128)(2,1)S(1)} %copy-done.4, f32[1,2048]{1,0:T(1,128)S(1)} %bitcast.14, s32[4,64]{1,0:T(4,128)S(1)} %bitcast.15, ...), custom_call_target="tpu_custom_call" | custom-call | tf_op jit(solution)/shard_map/project/pallas_call | solution.py:426
  90.8 39.3 %exchange.2 = bf16[128,8,1024]{2,1,0:T(8,128)(2,1)S(1)} custom-call(bf16[128,8,1024]{2,1,0:T(8,128)(2,1)S(1)} %bitcast.13), custom_call_target="tpu_custom_call" | custom-call | tf_op jit(solution)/shard_map/exchange/pallas_call | solution.py:384
  130.1 7.4 %experts.1 = bf16[1024,1024]{1,0:T(8,128)(2,1)S(1)} custom-call(bf16[1024,1024]{1,0:T(8,128)(2,1)S(1)} %bitcast.10, bf16[2048,512]{1,0:T(8,128)(2,1)} %bitcast.16, bf16[2048,512]{1,0:T(8,128)(2,1)} %bitcast.17, bf16[512,2048]{1,0:T(8,128)(2,1)} %bitcast.18), custom_call_target="tpu_custom_call" | custom-call | tf_op jit(solution)/shard_map/experts/pallas_call | solution.py:461
  137.5 0.0 copy-start.8
  137.5 32.8 %exchange.3 = bf16[128,8,1024]{2,1,0:T(8,128)(2,1)S(1)} custom-call(bf16[128,8,1024]{2,1,0:T(8,128)(2,1)S(1)} %bitcast.11), custom_call_target="tpu_custom_call" | custom-call | tf_op jit(solution)/shard_map/exchange/pallas_call | solution.py:384
  170.3 0.1 copy.18.routes_ref
  170.4 0.0 copy-done.8
  170.4 0.1 copy.19.score_ref
  170.5 1.8 %combine.1 = bf16[64,2048]{1,0:T(8,128)(2,1)} custom-call(bf16[1024,1024]{1,0:T(8,128)(2,1)S(1)} %bitcast.12, f32[64,2048]{1,0:T(8,128)S(1)} %get-tuple-element.12.base_ref, s32[64,4]{1,0:T(8,128)S(1)} %copy.18.routes_ref, f32[64,4]{1,0:T(8,128)S(1)} %copy.19.score_ref), custom_call_target="tpu_custom_call" | custom-call | tf_op jit(solution)/shard_map/combine/pallas_call | solution.py:503
Async XLA Ops:
  28.8 1.7 copy-start
  30.5 0.9 copy-start.5
  31.4 49.8 %copy-start.1 = (bf16[2048,512]{1,0:T(8,128)(2,1)S(1)}, bf16[2048,512]{1,0:T(8,128)(2,1)}, u32[]{:S(2)}) copy-start(bf16[2048,512]{1,0:T(8,128)(2,1)} %sg_ref.1) | copy-start | bytes 6291460
  31.4 49.8 %copy-start.4 = (bf16[64,2048]{1,0:T(8,128)(2,1)S(1)}, bf16[64,2048]{1,0:T(8,128)(2,1)}, u32[]{:S(2)}) copy-start(bf16[64,2048]{1,0:T(8,128)(2,1)} %stream_ref.1) | copy-start | bytes 786436
  31.4 49.8 %copy-start.6 = (f32[2048]{0:T(1024)S(1)}, f32[2048]{0:T(1024)}, u32[]{:S(2)}) copy-start(f32[2048]{0:T(1024)} %param.21) | copy-start | bytes 24580
  31.4 49.8 %copy-start.7 = (s32[64,4]{0,1:T(4,128)S(1)}, s32[64,4]{0,1:T(4,128)}, u32[]{:S(2)}) copy-start(s32[64,4]{0,1:T(4,128)} %param.22) | copy-start | bytes 3076
  72.5 0.7 copy-start.2
  81.3 1.0 copy-start.3
  137.5 32.9 %copy-start.8 = (f32[64,4]{0,1:T(4,128)S(1)}, f32[64,4]{0,1:T(4,128)}, u32[]{:S(2)}) copy-start(f32[64,4]{0,1:T(4,128)} %param.23) | copy-start | bytes 3076

commit v2 on v1

--- a/solution.py
+++ b/solution.py
@@ -288,24 +288,54 @@
     )(mine, queries)
 
 
-def swap_kernel(thresholds, att_ref, out_ref, send, recv):
+def offsets():
+    every = [(dz, dy, dx, dc) for dz in range(4) for dy in range(4) for dx in range(4) for dc in range(2)][1:]
+    order = np.random.default_rng(1).permutation(len(every))
+    return [every[k] for k in order]
+
+
+def slot_codes(shape, dim):
+    at = lax.broadcasted_iota(jnp.int32, shape, dim)
+    return at // 8, at // 4 % 2, at % 4
+
+
+GROUPS = 4
+
+
+def layer_kernel(
+    thresholds, att_ref, w_hbm, stream_ref, gain_ref, routes_ref, routes_t_ref, score_ref, sg_hbm, su_hbm, sd_hbm, g_hbm, u_hbm, d_hbm,
+    out_ref, w_ref, sg_ref, su_ref, sd_ref, g_ref, u_ref, d_ref, heads, leaving, arrived, done, back,
+    load, swap_send, swap_recv, go_send, go_recv, back_send, back_recv, own_sem,
+):
+    f32, bf16 = jnp.float32, jnp.bfloat16
+    dot = functools.partial(jnp.dot, preferred_element_type=f32)
     z, y, c, x = place()
     sp = (z * 4 + y) * 2 + c
+    me = sp * 4 + x
     other = 31 - sp
     n = given_tiles(sp, thresholds)
     low = sp < 16
+    steps = offsets()
+
+    def peer(o, way=1):
+        return (((z + way * o[0]) % 4 * 4 + (y + way * o[1]) % 4) * 2 + (c + o[3]) % 2, (x + way * o[2]) % 4)
+
     barrier = pltpu.get_barrier_semaphore()
-    for d in (1, 2, 3):
-        pl.semaphore_signal(barrier, inc=1, device_id=(sp, (x + d) % 4), device_id_type=MESH)
-    for d in range(4):
-        pl.semaphore_signal(barrier, inc=1, device_id=(other, (x + d) % 4), device_id_type=MESH)
-    pl.semaphore_wait(barrier, 7)
+    for o in steps:
+        pl.semaphore_signal(barrier, inc=1, device_id=peer(o), device_id_type=MESH)
+    loads = []
+    for k, (src, dst) in enumerate(
+        ((w_hbm, w_ref), (sg_hbm, sg_ref), (su_hbm, su_ref), (sd_hbm, sd_ref), (g_hbm, g_ref), (u_hbm, u_ref), (d_hbm, d_ref))
+    ):
+        loads.append(pltpu.make_async_copy(src, dst, load.at[k]))
+        loads[-1].start()
+    pl.semaphore_wait(barrier, len(steps))
 
     def tile(s):
         return att_ref.at[pl.ds(s * 32, 32), :]
 
     def spot(t, half):
-        return out_ref.at[t, pl.ds(half * 32, 32), :]
+        return heads.at[t, pl.ds(half * 32, 32), :]
 
     jobs = []
     for d in (1, 3, 2, 0):
@@ -313,164 +343,62 @@
             s = (x + d) % 4 * 2 + half
             made = jnp.logical_or(low, s >= n)
             if d == 0:
-                copy = pltpu.make_async_copy(tile(s), spot(x, half), recv.at[x * 2 + half])
+                copy = pltpu.make_async_copy(tile(s), spot(x, half), swap_recv.at[x * 2 + half])
             else:
                 copy = pltpu.make_async_remote_copy(
-                    src_ref=tile(s), dst_ref=spot(x, half), send_sem=send.at[d * 2 + half], recv_sem=recv.at[x * 2 + half],
+                    src_ref=tile(s), dst_ref=spot(x, half), send_sem=swap_send.at[d * 2 + half], recv_sem=swap_recv.at[x * 2 + half],
                     device_id=(sp, (x + d) % 4), device_id_type=MESH,
                 )
             jobs.append((made, copy, d != 0))
     for s in range(len(thresholds)):
         made = jnp.logical_and(low, s < n)
         copy = pltpu.make_async_remote_copy(
-            src_ref=tile(8 + s), dst_ref=spot(x, s % 2), send_sem=send.at[8 + s], recv_sem=recv.at[x * 2 + s % 2],
+            src_ref=tile(8 + s), dst_ref=spot(x, s % 2), send_sem=swap_send.at[8 + s], recv_sem=swap_recv.at[x * 2 + s % 2],
             device_id=(other, s // 2), device_id_type=MESH,
         )
         jobs.append((made, copy, True))
     for made, copy, _ in jobs:
         pl.when(made)(copy.start)
-    for t in range(4):
-        for half in (0, 1):
-            pltpu.make_async_copy(spot(t, half), spot(t, half), recv.at[t * 2 + half]).wait()
-    for made, copy, remote in jobs:
-        if remote:
-            pl.when(made)(copy.wait_send)
-
-
-def swap(att, thresholds):
-    return pl.pallas_call(
-        functools.partial(swap_kernel, thresholds),
-        out_shape=jax.ShapeDtypeStruct((4, 64, 512), jnp.bfloat16),
-        in_specs=[VM],
-        out_specs=VM,
-        scratch_shapes=[pltpu.SemaphoreType.DMA((12,)), pltpu.SemaphoreType.DMA((8,))],
-        compiler_params=pltpu.CompilerParams(collective_id=1, has_side_effects=True),
-        name="swap",
-    )(att)
-
-
-def offsets():
-    every = [(dz, dy, dx, dc) for dz in range(4) for dy in range(4) for dx in range(4) for dc in range(2)][1:]
-    order = np.random.default_rng(1).permutation(len(every))
-    return [every[k] for k in order]
-
-
-def exchange_kernel(x_ref, o_ref, send, recv, local):
-    z, y, c, x = place()
-    me = ((z * 4 + y) * 2 + c) * 4 + x
-
-    def peer(o):
-        return (((z + o[0]) % 4 * 4 + (y + o[1]) % 4) * 2 + (c + o[3]) % 2, (x + o[2]) % 4)
-
-    steps = offsets()
-    barrier = pltpu.get_barrier_semaphore()
-    for o in steps:
-        pl.semaphore_signal(barrier, inc=1, device_id=peer(o), device_id_type=MESH)
-    own = pltpu.make_async_copy(x_ref.at[me], o_ref.at[me], local)
-    own.start()
-    pl.semaphore_wait(barrier, len(steps))
-    for o in steps:
-        s, t = peer(o)
-        pltpu.make_async_remote_copy(
-            src_ref=x_ref.at[s * 4 + t], dst_ref=o_ref.at[me], send_sem=send, recv_sem=recv, device_id=(s, t), device_id_type=MESH
-        ).start()
-    own.wait()
-    count = len(steps)
-    pltpu.make_async_copy(x_ref.at[pl.ds(0, count)], o_ref.at[pl.ds(0, count)], send).wait()
-    pltpu.make_async_copy(x_ref.at[pl.ds(0, count)], o_ref.at[pl.ds(0, count)], recv).wait()
-
-
-def exchange(x, number):
-    return pl.pallas_call(
-        exchange_kernel,
-        out_shape=jax.ShapeDtypeStruct(x.shape, x.dtype),
-        in_specs=[VM],
-        out_specs=VM,
-        scratch_shapes=[pltpu.SemaphoreType.DMA] * 3,
-        compiler_params=pltpu.CompilerParams(collective_id=number, has_side_effects=True, vmem_limit_bytes=32 * 1024 * 1024),
-        name="exchange",
-    )(x)
-
-
-def slot_codes(shape, dim):
-    at = lax.broadcasted_iota(jnp.int32, shape, dim)
-    return at // 8, at // 4 % 2, at % 4
-
-
-def project_kernel(th_ref, w_ref, stream_ref, gain_ref, routes_ref, sg_ref, su_ref, sd_ref, out_ref, base_ref):
-    f32, bf16 = jnp.float32, jnp.bfloat16
-    dot = functools.partial(jnp.dot, preferred_element_type=f32)
-    mixed = sum(dot(th_ref[t], w_ref[pl.ds(512 * t, 512), :]) for t in range(4))
-    resid = (stream_ref[...].astype(f32) + mixed).astype(bf16).astype(f32)
-    factor = lax.rsqrt(jnp.mean(resid * resid, axis=1, keepdims=True) + 1e-06)
-    normed = (resid * factor * gain_ref[...]).astype(bf16)
+
     expert = lax.broadcasted_iota(jnp.int32, (128, 64), 0)
     named = jnp.zeros((128, 64), f32)
     for k in range(4):
-        named = jnp.where(routes_ref[pl.ds(k, 1), :] == expert, 1.0, named)
+        named = jnp.where(routes_t_ref[pl.ds(k, 1), :] == expert, 1.0, named)
     earlier = lax.broadcasted_iota(jnp.int32, (64, 64), 0) < lax.broadcasted_iota(jnp.int32, (64, 64), 1)
     rank = dot(named.astype(bf16), earlier.astype(f32).astype(bf16))
-    e, h, k = slot_codes((1024, 128), 0)
+    e, _, _ = slot_codes((1024, 128), 0)
     spread = (e == lax.broadcasted_iota(jnp.int32, (1024, 128), 1)).astype(f32).astype(bf16)
     both = dot(spread, jnp.concatenate([named, rank], axis=1).astype(bf16))
     _, h, k = slot_codes((1024, 64), 0)
     taken = jnp.where(both[:, 64:] == k.astype(f32), both[:, :64], 0.0)
     pick = jnp.concatenate([jnp.where(h == 0, taken, 0.0), jnp.where(h == 1, taken, 0.0)], axis=1).astype(bf16)
-    out_ref[...] = dot(pick, jnp.concatenate([normed[:, :1024], normed[:, 1024:]], axis=0)).astype(bf16)
+
+    loads[0].wait()
+    for t in range(4):
+        for half in (0, 1):
+            pltpu.make_async_copy(spot(t, half), spot(t, half), swap_recv.at[t * 2 + half]).wait()
+    mixed = sum(dot(heads[t], w_ref[pl.ds(512 * t, 512), :]) for t in range(4))
+    resid = (stream_ref[...].astype(f32) + mixed).astype(bf16).astype(f32)
+    factor = lax.rsqrt(jnp.mean(resid * resid, axis=1, keepdims=True) + 1e-06)
+    normed = (resid * factor * gain_ref[...]).astype(bf16)
+    picked = dot(pick, jnp.concatenate([normed[:, :1024], normed[:, 1024:]], axis=0))
+    leaving[...] = picked.reshape(128, 8, 1024).astype(bf16)
+
+    size = 128 // GROUPS
+    places = list(range(len(steps) + 1))
+    for j, o in enumerate(steps):
+        s, t = peer(o)
+        pltpu.make_async_remote_copy(
+            src_ref=leaving.at[s * 4 + t], dst_ref=arrived.at[j], send_sem=go_send, recv_sem=go_recv.at[j // size],
+            device_id=(s, t), device_id_type=MESH,
+        ).start()
+    pltpu.make_async_copy(leaving.at[me], arrived.at[127], go_recv.at[GROUPS - 1]).start()
+
+    for k in (1, 2, 3):
+        loads[k].wait()
     gate = dot(normed, sg_ref[...])
     inner = (gate * jax.nn.sigmoid(gate) * dot(normed, su_ref[...])).astype(bf16)
-    base_ref[...] = resid + dot(inner, sd_ref[...])
-
-
-def project(th, w, stream, gain, routes_t, sg, su, sd):
-    return pl.pallas_call(
-        project_kernel,
-        out_shape=(jax.ShapeDtypeStruct((1024, 1024), jnp.bfloat16), jax.ShapeDtypeStruct((64, 2048), jnp.float32)),
-        in_specs=[VM] * 8,
-        out_specs=(VM, VM),
-        compiler_params=pltpu.CompilerParams(vmem_limit_bytes=48 * 1024 * 1024),
-        name="project",
-    )(th, w, stream, gain, routes_t, sg, su, sd)
-
-
-def expert_kernel(x_ref, g_ref, u_ref, d_ref, out_ref):
-    f32, bf16 = jnp.float32, jnp.bfloat16
-    dot = functools.partial(jnp.dot, preferred_element_type=f32)
-    top = lax.broadcasted_iota(jnp.int32, (16, 8, 1024), 1) < 4
-
-    def some(j, _):
-        rows = pl.ds(j * 256, 256)
-        wide = x_ref[rows, :].astype(f32).reshape(16, 2, 8, 1024)
-        a, b = wide[:, 0], wide[:, 1]
-        left = jnp.where(top, a, pltpu.roll(b, 4, 1)).reshape(128, 1024).astype(bf16)
-        right = jnp.where(top, pltpu.roll(a, 4, 1), b).reshape(128, 1024).astype(bf16)
-        gate = dot(left, g_ref[0:1024, :]) + dot(right, g_ref[1024:2048, :])
-        up = dot(left, u_ref[0:1024, :]) + dot(right, u_ref[1024:2048, :])
-        inner = (gate * jax.nn.sigmoid(gate) * up).astype(bf16)
-        lo = dot(inner, d_ref[:, 0:1024]).reshape(16, 8, 1024)
-        hi = dot(inner, d_ref[:, 1024:2048]).reshape(16, 8, 1024)
-        first = jnp.where(top, lo, pltpu.roll(hi, 4, 1))
-        second = jnp.where(top, pltpu.roll(lo, 4, 1), hi)
-        out_ref[rows, :] = jnp.stack([first, second], axis=1).reshape(256, 1024).astype(bf16)
-        return 0
-
-    lax.fori_loop(0, 4, some, 0)
-
-
-def experts(x, g, u, d):
-    return pl.pallas_call(
-        expert_kernel,
-        out_shape=jax.ShapeDtypeStruct((1024, 1024), jnp.bfloat16),
-        in_specs=[VM] * 4,
-        out_specs=VM,
-        compiler_params=pltpu.CompilerParams(vmem_limit_bytes=48 * 1024 * 1024),
-        name="experts",
-    )(x, g, u, d)
-
-
-def combine_kernel(back_ref, base_ref, routes_ref, score_ref, out_ref):
-    f32, bf16 = jnp.float32, jnp.bfloat16
-    dot = functools.partial(jnp.dot, preferred_element_type=f32)
+    base = resid + dot(inner, sd_ref[...])
     score = score_ref[...]
     gates = 2.5 * score / jnp.sum(score, axis=1, keepdims=True)
     expert = lax.broadcasted_iota(jnp.int32, (64, 128), 1)
@@ -483,31 +411,74 @@
     earlier = lax.broadcasted_iota(jnp.int32, (64, 64), 1) < lax.broadcasted_iota(jnp.int32, (64, 64), 0)
     rank = dot(earlier.astype(f32).astype(bf16), named.astype(bf16))
     high = gate.astype(bf16)
-    low = (gate - high.astype(f32)).astype(bf16)
+    small = (gate - high.astype(f32)).astype(bf16)
     e, _, _ = slot_codes((128, 1024), 1)
     spread = (e == lax.broadcasted_iota(jnp.int32, (128, 1024), 0)).astype(f32).astype(bf16)
-    wide = dot(jnp.concatenate([rank.astype(bf16), high, low], axis=0), spread)
+    wide = dot(jnp.concatenate([rank.astype(bf16), high, small], axis=0), spread)
     _, h, k = slot_codes((64, 1024), 1)
     mine = wide[0:64] == k.astype(f32)
     parts = []
     for half in (0, 1):
         for piece in (wide[64:128], wide[128:192]):
             parts.append(jnp.where(mine & (h == half), piece, 0.0))
-    total = dot(jnp.concatenate(parts, axis=0).astype(bf16), back_ref[...])
-    base = base_ref[...]
+    weigh = jnp.concatenate(parts, axis=0).astype(bf16)
+
+    for k in (4, 5, 6):
+        loads[k].wait()
+    top = lax.broadcasted_iota(jnp.int32, (size // 2, 8, 1024), 1) < 4
+    for q in range(GROUPS):
+        rows = pl.ds(q * size, size)
+        pltpu.make_async_copy(arrived.at[rows], arrived.at[rows], go_recv.at[q]).wait()
+        wide = arrived[rows].astype(f32).reshape(size // 2, 2, 8, 1024)
+        a, b = wide[:, 0], wide[:, 1]
+        left = jnp.where(top, a, pltpu.roll(b, 4, 1)).reshape(size * 4, 1024).astype(bf16)
+        right = jnp.where(top, pltpu.roll(a, 4, 1), b).reshape(size * 4, 1024).astype(bf16)
+        gate = dot(left, g_ref[0:1024, :]) + dot(right, g_ref[1024:2048, :])
+        up = dot(left, u_ref[0:1024, :]) + dot(right, u_ref[1024:2048, :])
+        inner = (gate * jax.nn.sigmoid(gate) * up).astype(bf16)
+        lo = dot(inner, d_ref[:, 0:1024]).reshape(size // 2, 8, 1024)
+        hi = dot(inner, d_ref[:, 1024:2048]).reshape(size // 2, 8, 1024)
+        first = jnp.where(top, lo, pltpu.roll(hi, 4, 1))
+        second = jnp.where(top, pltpu.roll(lo, 4, 1), hi)
+        done[rows] = jnp.stack([first, second], axis=1).reshape(size, 8, 1024).astype(bf16)
+        for j in range(q * size, (q + 1) * size):
+            if j < len(steps):
+                s, t = peer(steps[j], -1)
+                pltpu.make_async_remote_copy(
+                    src_ref=done.at[j], dst_ref=back.at[me], send_sem=back_send, recv_sem=back_recv,
+                    device_id=(s, t), device_id_type=MESH,
+                ).start()
+            else:
+                pltpu.make_async_copy(done.at[j], back.at[me], back_recv).start()
+
+    pltpu.make_async_copy(back, back, back_recv).wait()
+    total = dot(weigh, back[...].reshape(1024, 1024))
     out_ref[:, 0:1024] = (base[:, 0:1024] + total[0:64] + total[64:128]).astype(bf16)
     out_ref[:, 1024:2048] = (base[:, 1024:2048] + total[128:192] + total[192:256]).astype(bf16)
-
-
-def combine(back, base, routes, score):
+    for made, copy, remote in jobs:
+        if remote:
+            pl.when(made)(copy.wait_send)
+    count = pl.ds(0, len(steps))
+    pltpu.make_async_copy(leaving.at[count], arrived.at[count], go_send).wait()
+    pltpu.make_async_copy(done.at[count], back.at[count], back_send).wait()
+
+
+def layer(att, thresholds, w, stream, gain, routes, score, sg, su, sd, g, u, d):
+    bf16 = jnp.bfloat16
+    hbm = pl.BlockSpec(memory_space=pl.ANY)
+    chunk = pltpu.VMEM((128, 8, 1024), bf16)
+    dma = pltpu.SemaphoreType.DMA
     return pl.pallas_call(
-        combine_kernel,
-        out_shape=jax.ShapeDtypeStruct((64, 2048), jnp.bfloat16),
-        in_specs=[VM] * 4,
+        functools.partial(layer_kernel, thresholds),
+        out_shape=jax.ShapeDtypeStruct(stream.shape, bf16),
+        in_specs=[VM, hbm, VM, VM, VM, VM, VM, hbm, hbm, hbm, hbm, hbm, hbm],
         out_specs=VM,
-        compiler_params=pltpu.CompilerParams(vmem_limit_bytes=32 * 1024 * 1024),
-        name="combine",
-    )(back, base, routes, score)
+        scratch_shapes=[pltpu.VMEM(a.shape, bf16) for a in (w, sg, su, sd, g, u, d)]
+        + [pltpu.VMEM((4, 64, 512), bf16), chunk, chunk, chunk, chunk]
+        + [dma((7,)), dma((12,)), dma((8,)), dma, dma((GROUPS,)), dma, dma, dma],
+        compiler_params=pltpu.CompilerParams(collective_id=1, has_side_effects=True, vmem_limit_bytes=56 * 1024 * 1024),
+        name="layer",
+    )(att, w, stream, gain, routes, routes.T, score, sg, su, sd, g, u, d)
 
 
 def body(
@@ -519,14 +490,10 @@
     kv, theirs = gather(pack(key_value[:, 0, :], break_bias), queries)
     tab = lax.dynamic_index_in_dim(jnp.asarray(table), lax.axis_index("sp"), 0, keepdims=False)
     made = attend(tab, jnp.concatenate([queries, theirs], axis=0), kv, GROUP, diag_groups)
-    heads = swap(made, thresholds)
-    outgoing, base = project(
-        heads, out_proj, stream, ffn_gain.reshape(1, -1), routes.T, shared_gate, shared_up, shared_down
+    return layer(
+        made, thresholds, out_proj, stream, ffn_gain.reshape(1, -1), routes, route_score,
+        shared_gate, shared_up, shared_down, expert_gate[0], expert_up[0], expert_down[0],
     )
-    arrived = exchange(outgoing.reshape(128, 8, 1024), 2)
-    done = experts(arrived.reshape(1024, 1024), expert_gate[0], expert_up[0], expert_down[0])
-    back = exchange(done.reshape(128, 8, 1024), 3)
-    return combine(back.reshape(1024, 1024), base, routes, route_score)
 
 
 def solution(mesh):

time: 173 us -> 152 us (0.88)
  the two profiles are of different devices: /device:TPU:1 before, /device:TPU:9 now
where the time goes in v2:
time: 152 us; the launch traced here: 151 us
  Pallas kernels  142 us (93%)
  local copies, waits for them, and re-layouts  8.55 us (6%)
    pallas_call x1, Pallas kernels, layer(): pl.pallas_call(functools.partial(layer_kernel, thresholds), out_shape=jax...  81.7 us
    pallas_call x1, Pallas kernels, attend(): pl.pallas_call(functools.partial(attend_kernel, group, ld), out_shape=jax...  36 us
    pallas_call x1, Pallas kernels, gather(): pl.pallas_call(gather_kernel, out_shape=(jax.ShapeDtypeStruct((32, 144, 2...  22.2 us
    unnamed x14, local copies, waits for them, and re-layouts  7.82 us

profile of v2, /device:TPU:9, one launch (start us, length us, event | category | flops | bytes accessed | tf_op | source)
XLA Modules:
  0.0 151.3 jit_solution(8525901130244920263)
XLA Ops:
  0.0 0.7 dynamic-slice_reduce_fusion.tab
  0.7 1.4 copy.17.bias_ref
  2.1 1.6 %pack.1.mine_ref = bf16[144,256]{1,0:T(8,128)(2,1)} custom-call(bf16[256,128]{1,0:T(8,128)(2,1)} %bitcast.9, bf16[256,8]{1,0:T(8,128)(2,1)} %copy.17.bias_ref), custom_call_target="tpu_custom_call" | custom-call | tf_op jit(solution)/shard_map/pack/pallas_call | solution.py:169
  3.8 22.2 %gather.1 = (bf16[32,144,256]{2,1,0:T(8,128)(2,1)}, bf16[128,512]{1,0:T(8,128)(2,1)}) custom-call(bf16[144,256]{1,0:T(8,128)(2,1)} %pack.1.mine_ref, bf16[256,512]{1,0:T(8,128)(2,1)} %q_ref.1), custom_call_target="tpu_custom_call" | custom-call | tf_op jit(solution)/shard_map/gather/pallas_call | solution.py:272
  26.0 0.0 copy-start.3
  26.0 0.0 copy-start.4
  26.0 1.1 pad_maximum_fusion.q_ref
  27.1 0.0 copy-start
  27.1 1.7 %copy-done = bf16[32,144,256]{2,1,0:T(8,128)(2,1)S(1)} copy-done((bf16[32,144,256]{2,1,0:T(8,128)(2,1)S(1)}, bf16[32,144,256]{2,1,0:T(8,128)(2,1)}, u32[]{:S(2)}) %copy-start) | copy-done | bytes 2359320
  28.8 0.0 copy-start.2
  28.8 0.9 copy-done.2
  29.7 36.0 %attend.1.att_ref = bf16[384,512]{1,0:T(8,128)(2,1)S(1)} custom-call(s32[322]{0:T(512)S(1)} %dynamic-slice_reduce_fusion.tab, bf16[384,512]{1,0:T(8,128)(2,1)S(1)} %pad_maximum_fusion.q_ref, bf16[32,144,256]{2,1,0:T(8,128)(2,1)S(1)} %copy-done, bf16[256,384]{1,0:T(8,128)(2,1)S(1)} %copy-done.2), custom_call_target="tpu_custom_call" | custom-call | tf_op jit(solution)/shard_map/attend/pallas_call | solution.py:126
  65.7 0.0 copy-start.1
  65.7 0.7 copy-done.1
  66.4 0.0 copy-done.3
  66.5 0.7 copy.18.routes_ref
  67.2 0.0 copy-done.4
  67.2 0.7 copy.19.score_ref
  67.9 81.7 %layer.1 = bf16[64,2048]{1,0:T(8,128)(2,1)} custom-call(bf16[384,512]{1,0:T(8,128)(2,1)} %copy-done.1, bf16[2048,2048]{1,0:T(8,128)(2,1)} %w_hbm.1, bf16[64,2048]{1,0:T(8,128)(2,1)} %stream_ref.1, f32[1,2048]{1,0:T(1,128)} %bitcast.10, s32[64,4]{1,0:T(8,128)} %copy.18.routes_ref, s32[4,64]{1,0:T(4,128)} %bitcast.11, f32[64,4]{1,0:T(8,128)} %copy.19.score_ref, ...), custom_call_target="tpu_custom_call" | custom-call | tf_op jit(solution)/shard_map/layer/pallas_call | solution.py:471
  149.6 1.7 %copy.21 = bf16[64,2048]{1,0:T(8,128)(2,1)} copy(bf16[64,2048]{1,0:T(8,128)(2,1)} %layer.1) | data formatting | bytes 524288
Async XLA Ops:
  26.0 40.4 %copy-start.3 = (s32[64,4]{0,1:T(4,128)S(1)}, s32[64,4]{0,1:T(4,128)}, u32[]{:S(2)}) copy-start(s32[64,4]{0,1:T(4,128)} %param.22) | copy-start | bytes 3076
  26.0 41.1 %copy-start.4 = (f32[64,4]{0,1:T(4,128)S(1)}, f32[64,4]{0,1:T(4,128)}, u32[]{:S(2)}) copy-start(f32[64,4]{0,1:T(4,128)} %param.23) | copy-start | bytes 3076
  27.1 1.7 %copy-start = (bf16[32,144,256]{2,1,0:T(8,128)(2,1)S(1)}, bf16[32,144,256]{2,1,0:T(8,128)(2,1)}, u32[]{:S(2)}) copy-start(bf16[32,144,256]{2,1,0:T(8,128)(2,1)} %get-tuple-element.8.kv_ref) | copy-start | bytes 7077892
  28.8 0.9 copy-start.2
  65.7 0.8 copy-start.1

commit v3 on v2

--- a/solution.py
+++ b/solution.py
@@ -8,98 +8,118 @@
 from jax.experimental.pallas import tpu as pltpu
 from jax.sharding import PartitionSpec as P
 
-GROUP = 8
+GROUP = 4
 LOG2E = 1.4426950408889634
 
 
 def schedule(blocks, tiles, group):
     half = blocks // 2
-    rows = []
     give = []
     for i in range(half):
-        best = min(range(0, tiles // 2 + 1), key=lambda n: max(tiles * (i + 1) + n * (blocks - i), (tiles - n) * (blocks - i)))
-        give.append(best)
+        give.append(min(range(tiles // 2 + 1), key=lambda n: max(tiles * (i + 1) + n * (blocks - i), (tiles - n) * (blocks - i))))
+    spare = tiles + tiles // 2
+    lists = []
     for i in range(blocks):
         n = give[min(i, blocks - 1 - i)]
         if i < half:
             slots = [(s, i) for s in range(tiles)] + [(tiles + s, blocks - 1 - i) for s in range(n)]
         else:
             slots = [(s, i) for s in range(n, tiles)]
-        diag = [(s, q) for s, q in slots]
-        main = []
-        depth = max(q for _, q in slots)
-        for back in range(1, depth + 1):
-            for s, q in slots:
-                if q - back >= 0:
-                    main.append((s, q - back))
-        rows.append((diag, main))
-    spare = tiles + tiles // 2
-    ld = max(-(-len(d) // group) for d, _ in rows)
-    lm = max(-(-len(m) // group) for _, m in rows)
-    table = np.zeros((blocks, 2 + 2 * group * (ld + lm)), np.int32)
-    for i, (diag, main) in enumerate(rows):
-        nd, nm = -(-len(diag) // group), -(-len(main) // group)
-        diag = diag + [(spare, 0)] * (group * ld - len(diag))
-        main = main + [(spare, 0)] * (group * lm - len(main))
-        table[i, 0], table[i, 1] = nd, nm
-        table[i, 2:] = np.array(diag + main).reshape(-1)
-    return table, np.array(give), ld, lm
-
-
-def attend_kernel(group, ld, tab, q_ref, kv_ref, tri_ref, out_ref, qs, acc, carry):
+        left = {s: q + 1 for s, q in slots}
+        own = dict(slots)
+        groups = []
+        while any(left.values()):
+            chosen = sorted((s for s in left if left[s]), key=lambda s: -left[s])[:group]
+            cells = []
+            for s in chosen:
+                back = own[s] + 1 - left[s]
+                cells.append((s, own[s] - back, 256 * back + 32 * (s % tiles)))
+                left[s] -= 1
+            groups.append(cells + [(spare, 0, 0)] * (group - len(cells)))
+        lists.append(groups)
+    longest = max(len(g) for g in lists)
+    table = np.zeros((blocks, 1 + 3 * group * (longest + 3)), np.int32)
+    for i, groups in enumerate(lists):
+        table[i, 0] = -(-len(groups) // 2)
+        flat = groups + [[(spare, 0, 0)] * group] * (longest + 3 - len(groups))
+        table[i, 1:] = np.array(flat).reshape(-1)
+    return table, np.array(give)
+
+
+def attend_kernel(group, tab, q_ref, more_ref, kv_ref, tri_ref, out_ref, qs, acc, carry, gap, ub, sb):
     nt = out_ref.shape[0] // 32
+    sp = lax.axis_index("sp")
     f32, bf16 = jnp.float32, jnp.bfloat16
-    head_lane = lax.broadcasted_iota(jnp.int32, (32, 16), 1)
+    head_lane = lax.broadcasted_iota(jnp.int32, (32, 128), 1)
     c_hi = float(np.asarray(LOG2E, jnp.bfloat16))
     c_lo = float(np.float32(LOG2E - c_hi))
 
-    def build(s, _):
-        q = q_ref[pl.ds(s * 32, 32), :].astype(f32) * (0.125 * LOG2E)
+    def build(ref, base, s, _):
+        q = ref[pl.ds(s * 32, 32), :].astype(f32) * (0.125 * LOG2E)
+        s = s + base
         hi = q.astype(bf16)
         lo = (q - hi.astype(f32)).astype(bf16)
         for h in range(8):
             tail = jnp.where(head_lane == h, c_hi, jnp.where(head_lane == h + 8, c_lo, 0.0)).astype(bf16)
             qs[s, pl.ds(h * 32, 32), :] = jnp.concatenate([hi[:, 64 * h:64 * h + 64], lo[:, 64 * h:64 * h + 64], tail], axis=1)
+        acc[s] = jnp.zeros((256, 128), f32)
+        carry[s] = jnp.zeros((256, 128), f32)
         return 0
 
-    lax.fori_loop(0, nt, build, 0)
+    lax.fori_loop(0, nt * 2 // 3, functools.partial(build, q_ref, 0), 0)
+    lax.fori_loop(0, nt // 3, functools.partial(build, more_ref, nt * 2 // 3), 0)
     qs[nt] = jnp.zeros_like(qs[nt])
-    acc[...] = jnp.zeros_like(acc)
-    carry[...] = jnp.zeros_like(carry)
+    acc[nt] = jnp.zeros((256, 128), f32)
+    carry[nt] = jnp.zeros((256, 128), f32)
+    gap[...] = lax.broadcasted_iota(jnp.int32, (256, 256), 1) - lax.broadcasted_iota(jnp.int32, (256, 256), 0) % 32
     lane = lax.broadcasted_iota(jnp.int32, (128, 128), 1)
-
-    def step(base, masked):
+    blank = jnp.zeros((112, 256), bf16)
+    last = lax.broadcasted_iota(jnp.int32, (256, 128), 1) == 127
+
+    def cell(k, g):
+        at = 1 + 3 * (group * k + g)
+        return tab[sp, at], tab[sp, at + 1], tab[sp, at + 2]
+
+    def first(k, buf):
         for g in range(group):
-            slot = tab[base + 2 * g]
-            chunk = tab[base + 2 * g + 1]
-            key = jnp.concatenate([kv_ref[chunk, 0:64, :], kv_ref[chunk, 0:80, :]], axis=0)
+            slot, chunk, bound = cell(k, g)
+            key = jnp.concatenate([kv_ref[chunk, 0:64, :], kv_ref[chunk, 0:80, :], blank], axis=0)
             z = jnp.dot(qs[slot], key, preferred_element_type=f32)
-            if masked:
-                row = lax.broadcasted_iota(jnp.int32, (256, 256), 0) % 32 + (slot % 8) * 32
-                col = lax.broadcasted_iota(jnp.int32, (256, 256), 1)
-                z = jnp.where(col < row, z, -1e30)
-            sp = jnp.maximum(z, lax.log2(1.0 + jnp.exp2(jnp.minimum(z, 126.0))))
-            u = z - sp
-            sums = jnp.dot(sp.astype(bf16), tri_ref[...], preferred_element_type=f32)
-            before = carry[slot]
-            w = jnp.exp2(u - sums[:, :256] - jnp.concatenate([before, before], axis=1)).astype(bf16)
-            carry[slot] = before + sums[:, 256:]
+            z = jnp.where(gap[...] < bound, z, -1e30)
+            stay = jnp.maximum(z, lax.log2(1.0 + jnp.exp2(jnp.minimum(z, 126.0))))
+            ub[buf, g] = z - stay
+            sb[buf, g] = stay.astype(bf16)
+
+    def second(k, buf):
+        cells = [cell(k, g) for g in range(group)]
+        before = [carry[slot] for slot, _, _ in cells]
+        for g, (slot, chunk, _) in enumerate(cells):
+            sums = jnp.dot(sb[buf, g], tri_ref[...], preferred_element_type=f32)
+            late = sums[:, 128:]
+            w = jnp.concatenate(
+                [
+                    jnp.exp2(ub[buf, g, :, :128] - sums[:, :128] - before[g]).astype(bf16),
+                    jnp.exp2(ub[buf, g, :, 128:] - jnp.where(last, 0.0, late) - before[g]).astype(bf16),
+                ],
+                axis=1,
+            )
+            carry[slot] = before[g] + jnp.broadcast_to(late[:, 127:128], (256, 128))
             vx = kv_ref[chunk, 80:144, :]
             v = jnp.concatenate([vx[:, :128], vx[:, 128:]], axis=0)
             zero = jnp.zeros_like(v)
             both = jnp.concatenate([jnp.where(lane < 64, v, zero), jnp.where(lane < 64, zero, v)], axis=0)
             acc[slot] += jnp.dot(w, both, preferred_element_type=f32)
 
-    def diag_step(j, _):
-        step(2 + 2 * group * j, True)
+    first(0, 0)
+
+    def step(j, _):
+        first(2 * j + 1, 1)
+        second(2 * j, 0)
+        first(2 * j + 2, 0)
+        second(2 * j + 1, 1)
         return 0
 
-    def main_step(j, _):
-        step(2 + 2 * group * (ld + j), False)
-        return 0
-
-    lax.fori_loop(0, tab[0], diag_step, 0)
-    lax.fori_loop(0, tab[1], main_step, 0)
+    lax.fori_loop(0, tab[sp, 0], step, 0)
 
     def finish(s, _):
         for p in range(4):
@@ -114,24 +134,32 @@
 
 
 def triangle():
-    t = np.zeros((256, 384), np.float32)
-    t[:, :256] = np.tril(np.ones((256, 256)), -1)
-    t[:, 256:] = 1.0
+    t = np.tril(np.ones((256, 256), np.float32), -1)
+    t[:, 255] = 1.0
     return t
 
 
-def attend(tab, q_all, kv, group, ld):
-    nt = q_all.shape[0] // 32
+def attend(tab, queries, more, kv, group):
+    nt = (queries.shape[0] + more.shape[0]) // 32
     vm = pl.BlockSpec(memory_space=pltpu.VMEM)
+    tile = pltpu.VMEM((nt + 1, 256, 128), jnp.float32)
     return pl.pallas_call(
-        functools.partial(attend_kernel, group, ld),
-        out_shape=jax.ShapeDtypeStruct(q_all.shape, jnp.bfloat16),
-        in_specs=[pl.BlockSpec(memory_space=pltpu.SMEM), vm, vm, vm],
+        functools.partial(attend_kernel, group),
+        out_shape=jax.ShapeDtypeStruct((nt * 32, queries.shape[1]), jnp.bfloat16),
+        in_specs=[pl.BlockSpec(memory_space=pltpu.SMEM), vm, vm, vm, vm],
         out_specs=vm,
-        scratch_shapes=[pltpu.VMEM((nt + 1, 256, 144), jnp.bfloat16), pltpu.VMEM((nt + 1, 256, 128), jnp.float32), pltpu.VMEM((nt + 1, 256, 128), jnp.float32)],
-        compiler_params=pltpu.CompilerParams(vmem_limit_bytes=48 * 1024 * 1024),
+        scratch_shapes=[
+            pltpu.VMEM((nt + 1, 256, 256), jnp.bfloat16),
+            tile,
+            tile,
+            pltpu.VMEM((256, 256), jnp.int32),
+            pltpu.VMEM((2, group, 256, 256), jnp.float32),
+            pltpu.VMEM((2, group, 256, 256), jnp.bfloat16),
+        ],
+        compiler_params=pltpu.CompilerParams(vmem_limit_bytes=28 * 1024 * 1024),
+        cost_estimate=pl.CostEstimate(flops=2 * 10**10, bytes_accessed=3 * 10**6, transcendentals=2 * 10**7),
         name="attend",
-    )(tab, q_all, kv, jnp.asarray(triangle(), jnp.bfloat16))
+    )(tab, queries, more, kv, jnp.asarray(triangle(), jnp.bfloat16))
 
 
 MESH = pl.DeviceIdType.MESH
@@ -155,7 +183,7 @@
     f32, bf16 = jnp.float32, jnp.bfloat16
     kv = kv_ref[...].astype(f32)
     keys = kv.T[0:64].astype(bf16)
-    shift = jnp.concatenate([bias_ref[...].astype(f32), jnp.zeros((256, 120), f32)], axis=1).T[0:8]
+    shift = bias_ref[...].astype(f32)
     shifts = jnp.concatenate([shift, shift], axis=0).astype(bf16)
     v = kv[:, 64:]
     left = jnp.concatenate([v[0:64], v[128:192]], axis=1)
@@ -171,8 +199,10 @@
         out_shape=jax.ShapeDtypeStruct((144, 256), jnp.bfloat16),
         in_specs=[VM, VM],
         out_specs=VM,
+        compiler_params=pltpu.CompilerParams(vmem_limit_bytes=8 * 1024 * 1024),
+        cost_estimate=pl.CostEstimate(flops=10**8, bytes_accessed=10**5, transcendentals=0),
         name="pack",
-    )(key_value, bias)
+    )(key_value, bias.T)
 
 
 def gather_kernel(mine_ref, q_ref, kv_ref, theirs_ref, send, recv_a, recv_b, recv_s, q_send, q_recv, local):
@@ -283,7 +313,8 @@
             pltpu.SemaphoreType.DMA,
             pltpu.SemaphoreType.DMA,
         ],
-        compiler_params=pltpu.CompilerParams(collective_id=0, has_side_effects=True),
+        compiler_params=pltpu.CompilerParams(collective_id=0, has_side_effects=True, vmem_limit_bytes=16 * 1024 * 1024),
+        cost_estimate=pl.CostEstimate(flops=10**10, bytes_accessed=3 * 10**6, transcendentals=0),
         name="gather",
     )(mine, queries)
 
@@ -303,9 +334,9 @@
 
 
 def layer_kernel(
-    thresholds, att_ref, w_hbm, stream_ref, gain_ref, routes_ref, routes_t_ref, score_ref, sg_hbm, su_hbm, sd_hbm, g_hbm, u_hbm, d_hbm,
+    thresholds, att_ref, w_hbm, stream_ref, gain_ref, routes_ref, score_ref, sg_hbm, su_hbm, sd_hbm, g_hbm, u_hbm, d_hbm,
     out_ref, w_ref, sg_ref, su_ref, sd_ref, g_ref, u_ref, d_ref, heads, leaving, arrived, done, back,
-    load, swap_send, swap_recv, go_send, go_recv, back_send, back_recv, own_sem,
+    load, swap_send, swap_recv, go_send, go_recv, back_send, back_recv,
 ):
     f32, bf16 = jnp.float32, jnp.bfloat16
     dot = functools.partial(jnp.dot, preferred_element_type=f32)
@@ -363,7 +394,7 @@
     expert = lax.broadcasted_iota(jnp.int32, (128, 64), 0)
     named = jnp.zeros((128, 64), f32)
     for k in range(4):
-        named = jnp.where(routes_t_ref[pl.ds(k, 1), :] == expert, 1.0, named)
+        named = jnp.where(routes_ref[pl.ds(k, 1), :] == expert, 1.0, named)
     earlier = lax.broadcasted_iota(jnp.int32, (64, 64), 0) < lax.broadcasted_iota(jnp.int32, (64, 64), 1)
     rank = dot(named.astype(bf16), earlier.astype(f32).astype(bf16))
     e, _, _ = slot_codes((1024, 128), 0)
@@ -396,20 +427,16 @@
 
     for k in (1, 2, 3):
         loads[k].wait()
-    gate = dot(normed, sg_ref[...])
-    inner = (gate * jax.nn.sigmoid(gate) * dot(normed, su_ref[...])).astype(bf16)
+    lit = dot(normed, sg_ref[...])
+    inner = (lit * jax.nn.sigmoid(lit) * dot(normed, su_ref[...])).astype(bf16)
     base = resid + dot(inner, sd_ref[...])
     score = score_ref[...]
-    gates = 2.5 * score / jnp.sum(score, axis=1, keepdims=True)
-    expert = lax.broadcasted_iota(jnp.int32, (64, 128), 1)
-    named = jnp.zeros((64, 128), f32)
-    gate = jnp.zeros((64, 128), f32)
+    gates = 2.5 * score / jnp.sum(score, axis=0, keepdims=True)
+    gate = jnp.zeros((128, 64), f32)
     for k in range(4):
-        hit = routes_ref[:, k : k + 1] == expert
-        named = jnp.where(hit, 1.0, named)
-        gate = jnp.where(hit, gates[:, k : k + 1], gate)
-    earlier = lax.broadcasted_iota(jnp.int32, (64, 64), 1) < lax.broadcasted_iota(jnp.int32, (64, 64), 0)
-    rank = dot(earlier.astype(f32).astype(bf16), named.astype(bf16))
+        gate = jnp.where(routes_ref[pl.ds(k, 1), :] == expert, gates[k : k + 1, :], gate)
+    turned = jnp.concatenate([rank, gate], axis=1).T
+    rank, gate = turned[0:64], turned[64:128]
     high = gate.astype(bf16)
     small = (gate - high.astype(f32)).astype(bf16)
     e, _, _ = slot_codes((128, 1024), 1)
@@ -465,31 +492,31 @@
 
 def layer(att, thresholds, w, stream, gain, routes, score, sg, su, sd, g, u, d):
     bf16 = jnp.bfloat16
-    hbm = pl.BlockSpec(memory_space=pl.ANY)
+    hbm = pl.BlockSpec(memory_space=pltpu.HBM)
     chunk = pltpu.VMEM((128, 8, 1024), bf16)
     dma = pltpu.SemaphoreType.DMA
     return pl.pallas_call(
         functools.partial(layer_kernel, thresholds),
         out_shape=jax.ShapeDtypeStruct(stream.shape, bf16),
-        in_specs=[VM, hbm, VM, VM, VM, VM, VM, hbm, hbm, hbm, hbm, hbm, hbm],
+        in_specs=[VM, hbm, VM, VM, VM, VM, hbm, hbm, hbm, hbm, hbm, hbm],
         out_specs=VM,
         scratch_shapes=[pltpu.VMEM(a.shape, bf16) for a in (w, sg, su, sd, g, u, d)]
         + [pltpu.VMEM((4, 64, 512), bf16), chunk, chunk, chunk, chunk]
-        + [dma((7,)), dma((12,)), dma((8,)), dma, dma((GROUPS,)), dma, dma, dma],
-        compiler_params=pltpu.CompilerParams(collective_id=1, has_side_effects=True, vmem_limit_bytes=56 * 1024 * 1024),
+        + [dma((7,)), dma((12,)), dma((8,)), dma, dma((GROUPS,)), dma, dma],
+        compiler_params=pltpu.CompilerParams(collective_id=1, has_side_effects=True, vmem_limit_bytes=46 * 1024 * 1024),
+        cost_estimate=pl.CostEstimate(flops=4 * 10**10, bytes_accessed=3 * 10**7, transcendentals=0),
         name="layer",
-    )(att, w, stream, gain, routes, routes.T, score, sg, su, sd, g, u, d)
+    )(att, w, stream, gain, routes.T, score.T, sg, su, sd, g, u, d)
 
 
 def body(
     queries, key_value, break_bias, stream, out_proj, ffn_gain, routes, route_score,
     expert_gate, expert_up, expert_down, shared_gate, shared_up, shared_down,
 ):
-    table, give, diag_groups, _ = schedule(lax.axis_size("sp"), queries.shape[0] // 32, GROUP)
+    table, give = schedule(lax.axis_size("sp"), queries.shape[0] // 32, GROUP)
     thresholds = tuple(int((give >= k).sum()) for k in range(1, int(give.max()) + 1))
     kv, theirs = gather(pack(key_value[:, 0, :], break_bias), queries)
-    tab = lax.dynamic_index_in_dim(jnp.asarray(table), lax.axis_index("sp"), 0, keepdims=False)
-    made = attend(tab, jnp.concatenate([queries, theirs], axis=0), kv, GROUP, diag_groups)
+    made = attend(jnp.asarray(table), queries, theirs, kv, GROUP)
     return layer(
         made, thresholds, out_proj, stream, ffn_gain.reshape(1, -1), routes, route_score,
         shared_gate, shared_up, shared_down, expert_gate[0], expert_up[0], expert_down[0],

time: 152 us -> 124 us (0.82)
  the two profiles are of different devices: /device:TPU:9 before, /device:TPU:1 now
where the time goes in v3:
time: 124 us; the launch traced here: 122 us
  Pallas kernels  119 us (96%)
  local copies, waits for them, and re-layouts  3.23 us (3%)
    pallas_call x1, Pallas kernels, layer(): pl.pallas_call(functools.partial(layer_kernel, thresholds), out_shape=jax...  67 us
    pallas_call x1, Pallas kernels, attend(): pl.pallas_call(functools.partial(attend_kernel, group), out_shape=jax.Sha...  30.2 us
    pallas_call x1, Pallas kernels, gather(): pl.pallas_call(gather_kernel, out_shape=(jax.ShapeDtypeStruct((32, 144, 2...  21.5 us
    unnamed x27, local copies, waits for them, and re-layouts  3.23 us

profile of v3, /device:TPU:1, one launch (start us, length us, event | category | flops | bytes accessed | tf_op | source)
XLA Modules:
  0.0 122.2 jit_solution(14549354399758160735)
XLA Ops:
  0.0 0.0 copy-start.6
  0.0 0.8 copy-done.6
  0.8 0.0 copy-start.8
  0.8 0.7 copy-done.8
  1.5 0.1 pack.1.mine_ref
  1.6 0.0 copy-start.3
  1.6 0.9 copy-done.3
  2.6 0.0 copy-start.4
  2.6 0.0 copy-start.11
  2.6 0.0 copy-start.12
  2.6 21.5 %gather.1 = (bf16[32,144,256]{2,1,0:T(8,128)(2,1)S(1)}, bf16[128,512]{1,0:T(8,128)(2,1)S(1)}) custom-call(bf16[144,256]{1,0:T(8,128)(2,1)S(1)} %pack.1.mine_ref, bf16[256,512]{1,0:T(8,128)(2,1)S(1)} %copy-done.3), custom_call_target="tpu_custom_call" | custom-call | flops 10000000000 | bytes 3000000 | tf_op jit(solution)/shard_map/gather/pallas_call | solution.py:302
  24.1 0.0 copy-done.4
  24.1 0.0 copy-done.11
  24.1 0.0 copy-done.12
  24.1 0.0 copy-start
  24.1 0.0 copy-start.1
  24.2 0.0 copy-start.2
  24.2 0.0 copy-start.5
  24.2 0.0 copy-start.7
  24.2 0.0 copy-start.9
  24.2 0.0 copy-start.10
  24.2 30.2 %attend.1.att_ref = bf16[384,512]{1,0:T(8,128)(2,1)S(1)} custom-call(s32[32,481]{1,0:T(8,128)S(1)} %copy-done.12, bf16[256,512]{1,0:T(8,128)(2,1)S(1)} %copy-done.4, bf16[128,512]{1,0:T(8,128)(2,1)S(1)} %get-tuple-element.7.more_ref, bf16[32,144,256]{2,1,0:T(8,128)(2,1)S(1)} %get-tuple-element.8.kv_ref, bf16[256,256]{1,0:T(8,128)(2,1)S(1)} %copy-done.11), custom_call_target="tpu_custom_call" | custom-call | flops 20000000000 | bytes 3000000 | tf_op jit(solution)/shard_map/attend/pallas_call | solution.py:146
  54.5 0.0 copy-done
  54.5 0.0 copy-done.1
  54.5 0.0 copy-done.2
  54.5 0.0 copy-done.5
  54.5 0.0 copy-done.7
  54.5 0.0 copy-done.9
  54.5 0.0 copy-done.10
  54.5 67.0 %layer.1 = bf16[64,2048]{1,0:T(8,128)(2,1)S(1)} custom-call(bf16[384,512]{1,0:T(8,128)(2,1)S(1)} %attend.1.att_ref, bf16[2048,2048]{1,0:T(8,128)(2,1)} %w_hbm.1, bf16[64,2048]{1,0:T(8,128)(2,1)S(1)} %copy-done.5, f32[1,2048]{1,0:T(1,128)S(1)} %bitcast.9, s32[4,64]{1,0:T(4,128)S(1)} %bitcast.11, f32[4,64]{1,0:T(4,128)S(1)} %bitcast.12, ...), custom_call_target="tpu_custom_call" | custom-call | flops 40000000000 | bytes 30000000 | tf_op jit(solution)/shard_map/layer/pallas_call | solution.py:498
  121.5 0.7 copy.18
Async XLA Ops:
  0.0 0.8 copy-start.6
  0.8 0.7 copy-start.8
  1.6 1.0 copy-start.3
  2.6 21.5 %copy-start.4 = (bf16[256,512]{1,0:T(8,128)(2,1)S(1)}, bf16[256,512]{1,0:T(8,128)(2,1)}, u32[]{:S(2)}) copy-start(bf16[256,512]{1,0:T(8,128)(2,1)} %q_ref.3) | copy-start | bytes 786436
  2.6 21.5 %copy-start.11 = (bf16[256,256]{1,0:T(8,128)(2,1)S(1)}, bf16[256,256]{1,0:T(8,128)(2,1)}, u32[]{:S(2)}) copy-start(bf16[256,256]{1,0:T(8,128)(2,1)} %constant.5.clone.tri_ref) | copy-start | bytes 393220
  2.6 21.6 %copy-start.12 = (s32[32,481]{1,0:T(8,128)S(1)}, s32[32,481]{1,0:T(8,128)}, u32[]{:S(2)}) copy-start(s32[32,481]{1,0:T(8,128)} %constant.4.clone.tab) | copy-start | bytes 184708
  24.1 30.3 %copy-start = (bf16[2048,512]{1,0:T(8,128)(2,1)S(1)}, bf16[2048,512]{1,0:T(8,128)(2,1)}, u32[]{:S(2)}) copy-start(bf16[2048,512]{1,0:T(8,128)(2,1)} %sg_hbm.1) | copy-start | bytes 6291460
  24.1 30.3 %copy-start.1 = (bf16[2048,512]{1,0:T(8,128)(2,1)S(1)}, bf16[2048,512]{1,0:T(8,128)(2,1)}, u32[]{:S(2)}) copy-start(bf16[2048,512]{1,0:T(8,128)(2,1)} %su_hbm.1) | copy-start | bytes 6291460
  24.2 30.3 %copy-start.2 = (bf16[512,2048]{1,0:T(8,128)(2,1)S(1)}, bf16[512,2048]{1,0:T(8,128)(2,1)}, u32[]{:S(2)}) copy-start(bf16[512,2048]{1,0:T(8,128)(2,1)} %sd_hbm.1) | copy-start | bytes 6291460
  24.2 30.3 %copy-start.5 = (bf16[64,2048]{1,0:T(8,128)(2,1)S(1)}, bf16[64,2048]{1,0:T(8,128)(2,1)}, u32[]{:S(2)}) copy-start(bf16[64,2048]{1,0:T(8,128)(2,1)} %stream_ref.1) | copy-start | bytes 786436
  24.2 30.3 %copy-start.7 = (f32[2048]{0:T(1024)S(1)}, f32[2048]{0:T(1024)}, u32[]{:S(2)}) copy-start(f32[2048]{0:T(1024)} %param.21) | copy-start | bytes 24580
  24.2 30.3 %copy-start.9 = (s32[64,4]{0,1:T(4,128)S(1)}, s32[64,4]{0,1:T(4,128)}, u32[]{:S(2)}) copy-start(s32[64,4]{0,1:T(4,128)} %param.22) | copy-start | bytes 3076
  24.2 30.3 %copy-start.10 = (f32[64,4]{0,1:T(4,128)S(1)}, f32[64,4]{0,1:T(4,128)}, u32[]{:S(2)}) copy-start(f32[64,4]{0,1:T(4,128)} %param.23) | copy-start | bytes 3076
